TPU v7x, 32 devices: a whole 2x2x4 slice. The times are simulated.
32 devices in a mesh: sp: 8 (over z, x), dp: 4 (over y, core).
Axes of the slice: x: 2, y: 2, z: 4, core: 2. Of those that a mesh axis runs over, the one named last changes fastest.
Arguments:
- residual_in: bfloat16 [4, 1024, 2048], P('dp', 'sp'), may hold values from -6 to 6
- query_proj: bfloat16 [4, 1024, 2048], P('dp', 'sp'), may hold values from -8 to 8
- key_proj: bfloat16 [4, 1024, 512], P('dp', 'sp'), may hold values from -8 to 8
- value_proj: bfloat16 [4, 1024, 512], P('dp', 'sp'), may hold values from -6 to 6
- query_gain: float32 [128], replicated, may hold values from 0.1 to 7
- key_gain: float32 [128], replicated, may hold values from 0.1 to 7
- out_weight: bfloat16 [2048, 2048], replicated, may hold values from -0.125 to 0.125
- post_gain: float32 [2048], replicated, may hold values from 0.1 to 1.9
- pre_gain: float32 [2048], replicated, may hold values from 0.1 to 1.9
- route_ids: int32 [4, 1024, 2], P('dp', 'sp'), may hold values from 0 to 31, as said below
- group_weight: float32 [4, 1024], P('dp', 'sp'), may hold values from 0.25 to 1
- first_share: float32 [4, 1024], P('dp', 'sp'), may hold values from 0.5 to 1
- gate_weight: bfloat16 [32, 2048, 512], P(('sp', 'dp')), may hold values from -0.125 to 0.125
- up_weight: bfloat16 [32, 2048, 512], P(('sp', 'dp')), may hold values from -0.125 to 0.125
- down_weight: bfloat16 [32, 512, 2048], P(('sp', 'dp')), may hold values from -0.25 to 0.25
Outputs:
- layer_out: bfloat16 [4, 1024, 2048], P('dp', 'sp')
Inputs may be any that keep to these rules, and one draw needn't show every extreme that they name: `route_ids`: each token names two different experts of one group of 8 consecutive experts. Among the 128 tokens of one device each group is chosen by exactly 32 tokens, no expert is named by more than 16 of them, and in every draw one expert of each group is named by exactly 16 tokens of every device.
All inputs are finite; a program needn't handle non-finite values.
Results may differ from a plain program's by a relative error of at most 0.009.
The roundings to bfloat16 on the way count: a program that leaves them out, or rounds other values in their place, can miss the bound.
Values may be sent and summed in bfloat16 or wider, within the bound.
A program may use at most 128 MiB of HBM per device.

v0:
```python
import functools

import jax
import jax.numpy as jnp
import numpy as np
from jax import lax
from jax.experimental import pallas as pl
from jax.experimental.pallas import tpu as pltpu
from jax.sharding import PartitionSpec as P

HEAD_DIM = 128
GRID_W = 64
GROUPS = 4
EPSILON = 1e-06
MESH = pl.DeviceIdType.MESH
VMEM_LIMIT = 60 * 1024 * 1024
F32 = jnp.float32
BF16 = jnp.bfloat16


def angle_tables(length):
    quarter = HEAD_DIM // 4
    inverse = 10000.0 ** (-np.arange(quarter, dtype=np.float64) / quarter)
    positions = np.arange(length)
    rows = (positions // GRID_W)[:, None] * inverse
    cols = (positions % GRID_W)[:, None] * inverse
    angles = np.concatenate([rows, rows, cols, cols], axis=-1)
    sign = np.where(np.arange(HEAD_DIM) % (2 * quarter) < quarter, -1.0, 1.0)
    return np.cos(angles).astype(np.float32), (np.sin(angles) * sign).astype(np.float32)


def rotate(raw, gain, cos, sin):
    floats = raw.astype(F32)
    normed = floats * lax.rsqrt(jnp.mean(floats * floats, axis=-1, keepdims=True) + EPSILON) * gain
    quarter = HEAD_DIM // 4
    lane = lax.broadcasted_iota(jnp.int32, normed.shape, 1)
    turned = jnp.where(
        (lane & (2 * quarter - 1)) < quarter,
        pltpu.roll(normed, HEAD_DIM - quarter, 1),
        pltpu.roll(normed, quarter, 1),
    )
    return (normed * cos + turned * sin).astype(BF16)


def remote(src, dst, send_sem, recv_sem, device):
    return pltpu.make_async_remote_copy(
        src_ref=src,
        dst_ref=dst,
        send_sem=send_sem,
        recv_sem=recv_sem,
        device_id=device,
        device_id_type=MESH,
    )


def attention_kernel(
    nz, nx,
    q_ref, k_ref, v_ref, qg_ref, kg_ref, cos_ref, sin_ref, res_ref, post_ref, pre_ref, ow_hbm,
    stream_ref, normed_ref,
    k_all, v_all, q_rot, k_rot, att, acc, ow, ow_sem,
    rk, rv, skx, sku, skd, svx, svu, svd,
):
    tokens, width = q_ref.shape
    heads = width // HEAD_DIM
    kv_heads = k_ref.shape[1] // HEAD_DIM
    group = heads // kv_heads
    me = lax.axis_index("sp")
    dp = lax.axis_index("dp")
    z, x = me // nx, me % nx
    up, down = (me + nx, dp), (me - nx, dp)
    has_up, has_down = z < nz - 1, z > 0
    both = ((k_ref, k_all, rk, skx, sku, skd), (v_ref, v_all, rv, svx, svu, svd))

    load_ow = pltpu.make_async_copy(ow_hbm, ow, ow_sem)
    load_ow.start()

    barrier = pltpu.get_barrier_semaphore()
    around = [(lax.rem(z + 1, nz) * nx + x, dp), (lax.rem(z + nz - 1, nz) * nx + x, dp)]
    beside = [(z * nx + lax.rem(x + off, nx), dp) for off in range(1, nx)]
    for device in around + beside:
        pl.semaphore_signal(barrier, inc=1, device_id=device, device_id_type=MESH)
    pl.semaphore_wait(barrier, len(around) + len(beside))

    def lanes_of(head):
        return pl.ds(pl.multiple_of(head * HEAD_DIM, HEAD_DIM), HEAD_DIM)

    def hop(src, buf, recv, send, slot, head, device):
        return remote(src, buf.at[slot, head], send, recv.at[slot, head], device)

    def send_own(head):
        for raw, buf, recv, sx, su, sd in both:
            src = raw.at[:, lanes_of(head)]

            @pl.when(has_up)
            def _():
                hop(src, buf, recv, su.at[me, head], me, head, up).start()

            @pl.when(has_down)
            def _():
                hop(src, buf, recv, sd.at[me, head], me, head, down).start()

        for raw, buf, recv, sx, su, sd in both:
            src = raw.at[:, lanes_of(head)]
            for off in range(1, nx):
                hop(src, buf, recv, sx.at[me, head, off], me, head, beside[off - 1]).start()

    def arrived(buf, recv, slot, head):
        block = buf.at[slot, head]
        remote(block, block, recv.at[slot, head], recv.at[slot, head], up).wait_recv()

    def relay(head):
        for dist in range(1, nz):
            for below in (True, False):
                source = z - dist if below else z + dist
                present = source >= 0 if below else source < nz
                further = has_up if below else has_down
                onward = up if below else down

                @pl.when(present)
                def _(source=source, below=below, further=further, onward=onward):
                    slot = source * nx + x
                    for _raw, buf, recv, sx, su, sd in both:
                        arrived(buf, recv, slot, head)
                        src = buf.at[slot, head]
                        send = su if below else sd

                        @pl.when(further)
                        def _(src=src, buf=buf, recv=recv, send=send):
                            hop(src, buf, recv, send.at[slot, head], slot, head, onward).start()

                        for off in range(1, nx):
                            hop(
                                src, buf, recv, sx.at[slot, head, off], slot, head,
                                beside[off - 1],
                            ).start()

    length = nz * nx * tokens
    factor = float(HEAD_DIM**-0.5 * np.log2(np.e))
    span = group * HEAD_DIM

    def attend(kv):
        for plane in range(nz):
            for off in range(1, nx):
                slot = plane * nx + lax.rem(x + off, nx)
                arrived(k_all, rk, slot, kv)
                arrived(v_all, rv, slot, kv)
        k_all[me, kv] = k_ref[:, lanes_of(kv)]
        v_all[me, kv] = v_ref[:, lanes_of(kv)]

        def place(slot, carry):
            rows = pl.ds(pl.multiple_of(slot * tokens, tokens), tokens)
            k_rot[rows, :] = rotate(k_all[slot, kv], kg_ref[...], cos_ref[rows, :], sin_ref[rows, :])
            return carry

        lax.fori_loop(0, nz * nx, place, 0)
        keys = k_rot[...]
        values = v_all[:, kv].reshape(length, HEAD_DIM)
        for member in range(group):
            scores = lax.dot_general(
                q_rot[kv * group + member], keys, (((1,), (1,)), ((), ())),
                preferred_element_type=F32,
            )
            top = jnp.max(scores, axis=-1, keepdims=True)
            raised = jnp.exp2((scores - top) * factor)
            probs = (raised * (1.0 / jnp.sum(raised, axis=-1, keepdims=True))).astype(BF16)
            att[:, member * HEAD_DIM : (member + 1) * HEAD_DIM] = jnp.dot(
                probs, values, preferred_element_type=F32
            ).astype(BF16)
        part = ow.at[pl.ds(pl.multiple_of(kv * span, span), span), :]
        tile = 1024
        for start in range(0, width, tile):
            columns = slice(start, start + tile)
            acc[:, columns] += jnp.dot(att[...], part[:, columns], preferred_element_type=F32)

    send_own(0)
    for head in range(1, min(3, kv_heads)):
        send_own(head)
    own = pl.multiple_of(me * tokens, tokens)
    q_cos = cos_ref[pl.ds(own, tokens), :]
    q_sin = sin_ref[pl.ds(own, tokens), :]
    for head in range(heads):
        q_rot[head] = rotate(
            q_ref[:, head * HEAD_DIM : (head + 1) * HEAD_DIM], qg_ref[...], q_cos, q_sin
        )
    acc[...] = jnp.zeros_like(acc)
    relay(0)
    load_ow.wait()

    def one_head(kv, carry):
        @pl.when(kv + 3 < kv_heads)
        def _():
            send_own(kv + 3)

        @pl.when(kv + 1 < kv_heads)
        def _():
            relay(kv + 1)

        attend(kv)
        return carry

    lax.fori_loop(0, kv_heads, one_head, 0)

    blend = acc[...].astype(BF16).astype(F32)
    blend = blend * lax.rsqrt(jnp.mean(blend * blend, axis=-1, keepdims=True) + EPSILON)
    stream = (res_ref[...].astype(F32) + blend * post_ref[...]).astype(BF16)
    stream_ref[...] = stream
    wide = stream.astype(F32)
    wide = wide * lax.rsqrt(jnp.mean(wide * wide, axis=-1, keepdims=True) + EPSILON)
    normed_ref[...] = (wide * pre_ref[...]).astype(BF16)

    def sent(buf, sem, device):
        block = buf.at[0, 0]
        remote(block, block, sem, sem, device).wait_send()

    def drain(head, carry):
        for _raw, buf, recv, sx, su, sd in both:
            for plane in range(nz):
                slot = plane * nx + x

                @pl.when(jnp.logical_and(has_up, z >= plane))
                def _(slot=slot):
                    sent(buf, su.at[slot, head], up)

                @pl.when(jnp.logical_and(has_down, z <= plane))
                def _(slot=slot):
                    sent(buf, sd.at[slot, head], down)

                for off in range(1, nx):
                    sent(buf, sx.at[slot, head, off], beside[off - 1])
        return carry

    lax.fori_loop(0, kv_heads, drain, 0)


def before(tokens):
    row = lax.broadcasted_iota(jnp.int32, (tokens, tokens), 0)
    col = lax.broadcasted_iota(jnp.int32, (tokens, tokens), 1)
    return (row < col).astype(F32).astype(BF16)


def group_choice(meta, first_expert, count, rows):
    tokens = meta.shape[1]
    low = first_expert.astype(F32)
    member = jnp.where((meta[0:1] >= low) & (meta[0:1] < low + float(count)), 1.0, 0.0)
    rank = jnp.dot(
        jnp.broadcast_to(member, (8, tokens)).astype(BF16),
        before(tokens),
        preferred_element_type=F32,
    )[0:1]
    place = lax.broadcasted_iota(jnp.int32, (rows, tokens), 0).astype(F32)
    return jnp.where(rank == place, 1.0, 0.0) * member


def slot_choice(meta, first_expert, count, cap):
    tokens = meta.shape[1]
    names = lax.broadcasted_iota(jnp.int32, (count, tokens), 0).astype(F32)
    names = names + first_expert.astype(F32)
    first = jnp.where(meta[0:1] == names, 1.0, 0.0)
    second = jnp.where(meta[1:2] == names, 1.0, 0.0)
    rank = jnp.dot((first + second).astype(BF16), before(tokens), preferred_element_type=F32)
    row = lax.broadcasted_iota(jnp.int32, (count * cap, count), 0)
    start = lax.broadcasted_iota(jnp.int32, (count * cap, count), 1) * cap
    widen = jnp.where((row >= start) & (row < start + cap), 1.0, 0.0).astype(BF16)

    def widened(values):
        return jnp.dot(widen, values.astype(BF16), preferred_element_type=F32)

    place = lax.broadcasted_iota(jnp.int32, (count * cap, tokens), 0) & (cap - 1)
    hit = jnp.where(widened(rank) == place.astype(F32), 1.0, 0.0)
    return widened(first) * hit, widened(second) * hit


def contract(left, right, dims):
    return lax.dot_general(
        left.astype(BF16), right.astype(BF16), ((dims[:1], dims[1:]), ((), ())),
        preferred_element_type=F32,
    )


def expert_kernel(
    nz, nx, n_dp,
    normed_ref, stream_ref, meta_ref, wg_hbm, wu_hbm, wd_hbm,
    out_ref,
    wg, wu, wd, w_sem, p1, r1, metas, p2, r2, o2, back, mix, fin,
    s1, t1, sm, tm, s2, t2, s3, t3, s4, t4,
):
    tokens, width = normed_ref.shape
    count, cap = p2.shape[1], p2.shape[2]
    rows = p1.shape[1]
    sp = lax.axis_index("sp")
    dp = lax.axis_index("dp")
    z, x = sp // nx, sp % nx
    me = x * n_dp + dp

    loads = [
        pltpu.make_async_copy(src, dst, w_sem.at[i])
        for i, (src, dst) in enumerate(((wg_hbm, wg), (wu_hbm, wu), (wd_hbm, wd)))
    ]
    for load in loads:
        load.start()

    def plane_peer(off):
        j = lax.rem(me + off, count)
        return j, (z * nx + j // n_dp, j % n_dp)

    def column_peer(dist):
        plane = lax.rem(z + dist, nz)
        return plane, (plane * nx + x, dp)

    barrier = pltpu.get_barrier_semaphore()
    for off in range(1, count):
        pl.semaphore_signal(barrier, inc=1, device_id=plane_peer(off)[1], device_id_type=MESH)
    for dist in range(1, nz):
        pl.semaphore_signal(barrier, inc=1, device_id=column_peer(dist)[1], device_id_type=MESH)

    meta = meta_ref[...]
    for g in range(nz):
        pick = group_choice(meta, jnp.int32(g * count), count, rows)
        p1[g] = contract(pick, normed_ref[...], (1, 0)).astype(BF16)
    metas[z] = meta
    r1[z] = p1[z]

    pl.semaphore_wait(barrier, count - 1 + nz - 1)
    for dist in range(1, nz):
        plane, device = column_peer(dist)
        remote(meta_ref, metas.at[z], sm.at[plane], tm.at[z], device).start()
        remote(p1.at[plane], r1.at[z], s1.at[plane], t1.at[z], device).start()

    first_expert = z * count

    def dispatch(dist, carry):
        source, device = column_peer(dist)

        @pl.when(dist > 0)
        def _():
            remote(meta_ref, metas.at[source], sm.at[source], tm.at[source], device).wait_recv()
            remote(p1.at[source], r1.at[source], s1.at[source], t1.at[source], device).wait_recv()

        got = metas[source]
        group = group_choice(got, first_expert, count, rows)
        first, second = slot_choice(got, first_expert, count, cap)
        pick = contract(first + second, group, (1, 1))
        packed = contract(pick, r1[source], (1, 0)).astype(BF16)
        p2[source] = packed.reshape(count, cap, width)
        r2[source, me] = p2[source, me]
        for off in range(1, count):
            j, device = plane_peer(off)
            remote(
                p2.at[source, j], r2.at[source, me], s2.at[source, j], t2.at[source, me], device
            ).start()
        return carry

    lax.fori_loop(0, nz, dispatch, 0)
    for load in loads:
        load.wait()

    def transform(dist, carry):
        source = lax.rem(z + dist + 1, nz)
        for off in range(1, count):
            j, device = plane_peer(off)
            remote(
                p2.at[source, j], r2.at[source, j], s2.at[source, j], t2.at[source, j], device
            ).wait_recv()
        arrived = r2[source].reshape(count * cap, width)
        gated = jnp.dot(arrived, wg[...], preferred_element_type=F32)
        lifted = jnp.dot(arrived, wu[...], preferred_element_type=F32)
        hidden = (gated / (1.0 + jnp.exp(-gated)) * lifted).astype(BF16)
        result = jnp.dot(hidden, wd[...], preferred_element_type=F32).astype(BF16)
        o2[source] = result.reshape(count, cap, width)
        back[source, me] = o2[source, me]
        for off in range(1, count):
            j, device = plane_peer(off)
            remote(
                o2.at[source, j], back.at[source, me], s3.at[source, j], t3.at[source, me], device
            ).start()
        return carry

    lax.fori_loop(0, nz, transform, 0)

    def combine(dist, carry):
        source, column = column_peer(dist + 1)
        for off in range(1, count):
            j, device = plane_peer(off)
            remote(
                o2.at[source, j], back.at[source, j], s3.at[source, j], t3.at[source, j], device
            ).wait_recv()
        got = metas[source]
        group = group_choice(got, first_expert, count, rows)
        first, second = slot_choice(got, first_expert, count, cap)
        outs = back[source].reshape(count * cap, width)
        one = contract(contract(group, first, (1, 1)), outs, (1, 0))
        two = contract(contract(group, second, (1, 1)), outs, (1, 0))
        weight = jnp.sum(group * got[2:3], axis=1, keepdims=True)
        share = jnp.sum(group * got[3:4], axis=1, keepdims=True)
        total = (weight * (share * one + (1.0 - share) * two)).astype(BF16)
        mix[source] = total

        @pl.when(dist == nz - 1)
        def _():
            fin[source] = total

        @pl.when(dist < nz - 1)
        def _():
            remote(mix.at[source], fin.at[z], s4.at[source], t4.at[z], column).start()

        return carry

    lax.fori_loop(0, nz, combine, 0)

    picks = [
        group_choice(meta, jnp.int32(g * count), count, rows) for g in range(nz)
    ]
    for dist in range(1, nz):
        plane, device = column_peer(dist)
        remote(mix.at[plane], fin.at[plane], s4.at[plane], t4.at[plane], device).wait_recv()
    every = jnp.concatenate(picks, axis=0)
    added = contract(every, fin[...].reshape(tokens, width), (0, 0))
    out_ref[...] = (stream_ref[...].astype(F32) + added).astype(BF16)

    for dist in range(1, nz):
        plane, device = column_peer(dist)
        remote(meta_ref, metas.at[z], sm.at[plane], tm.at[z], device).wait_send()
        remote(p1.at[plane], r1.at[z], s1.at[plane], t1.at[z], device).wait_send()
        remote(mix.at[plane], fin.at[z], s4.at[plane], t4.at[z], device).wait_send()

    def drain(source, carry):
        for off in range(1, count):
            j, device = plane_peer(off)
            remote(
                p2.at[source, j], r2.at[source, me], s2.at[source, j], t2.at[source, me], device
            ).wait_send()
            remote(
                o2.at[source, j], back.at[source, me], s3.at[source, j], t3.at[source, me], device
            ).wait_send()
        return carry

    lax.fori_loop(0, nz, drain, 0)


def local(
    residual_in, query_proj, key_proj, value_proj, query_gain, key_gain, out_weight, post_gain,
    pre_gain, route_ids, group_weight, first_share, gate_weight, up_weight, down_weight,
):
    n_sp = lax.axis_size("sp")
    n_dp = lax.axis_size("dp")
    tokens, width = query_proj.shape[1:]
    kv_width = key_proj.shape[2]
    heads, kv_heads = width // HEAD_DIM, kv_width // HEAD_DIM
    nz = GROUPS
    nx = n_sp // nz
    length = n_sp * tokens
    cos, sin = angle_tables(length)
    vmem = pl.BlockSpec(memory_space=pltpu.VMEM)
    hbm = pl.BlockSpec(memory_space=pl.ANY)
    dma = pltpu.SemaphoreType.DMA
    row = jax.ShapeDtypeStruct((tokens, width), BF16)
    stream, normed = pl.pallas_call(
        functools.partial(attention_kernel, nz, nx),
        out_shape=(row, row),
        in_specs=[vmem] * 10 + [hbm],
        out_specs=(vmem, vmem),
        scratch_shapes=[
            pltpu.VMEM((n_sp, kv_heads, tokens, HEAD_DIM), BF16),
            pltpu.VMEM((n_sp, kv_heads, tokens, HEAD_DIM), BF16),
            pltpu.VMEM((heads, tokens, HEAD_DIM), BF16),
            pltpu.VMEM((length, HEAD_DIM), BF16),
            pltpu.VMEM((tokens, width // kv_heads), BF16),
            pltpu.VMEM((tokens, width), F32),
            pltpu.VMEM((width, width), BF16),
            dma,
            dma((n_sp, kv_heads)), dma((n_sp, kv_heads)),
            dma((n_sp, kv_heads, nx)), dma((n_sp, kv_heads)), dma((n_sp, kv_heads)),
            dma((n_sp, kv_heads, nx)), dma((n_sp, kv_heads)), dma((n_sp, kv_heads)),
        ],
        compiler_params=pltpu.CompilerParams(
            collective_id=0, has_side_effects=True, vmem_limit_bytes=VMEM_LIMIT
        ),
        name="attention",
    )(
        query_proj[0], key_proj[0], value_proj[0],
        query_gain.reshape(1, -1), key_gain.reshape(1, -1),
        jnp.asarray(cos), jnp.asarray(sin),
        residual_in[0], post_gain.reshape(1, -1), pre_gain.reshape(1, -1), out_weight,
    )

    experts = gate_weight.shape[0] * n_sp * n_dp
    count = experts // nz
    cap = max(16, 4 * tokens // experts)
    rows = tokens // nz
    ff = gate_weight.shape[2]
    meta = jnp.concatenate(
        [route_ids[0].T.astype(F32), group_weight, first_share, jnp.zeros((4, tokens), F32)], axis=0
    )
    blocks = pltpu.VMEM((nz, count, cap, width), BF16)
    lines = pltpu.VMEM((nz, rows, width), BF16)
    out = pl.pallas_call(
        functools.partial(expert_kernel, nz, nx, n_dp),
        out_shape=row,
        in_specs=[vmem] * 3 + [hbm] * 3,
        out_specs=vmem,
        scratch_shapes=[
            pltpu.VMEM((width, ff), BF16),
            pltpu.VMEM((width, ff), BF16),
            pltpu.VMEM((ff, width), BF16),
            dma((3,)),
            lines, lines,
            pltpu.VMEM((nz, 8, tokens), F32),
            blocks, blocks, blocks, blocks,
            lines, lines,
            dma((nz,)), dma((nz,)), dma((nz,)), dma((nz,)),
            dma((nz, count)), dma((nz, count)), dma((nz, count)), dma((nz, count)),
            dma((nz,)), dma((nz,)),
        ],
        compiler_params=pltpu.CompilerParams(
            collective_id=1, has_side_effects=True, vmem_limit_bytes=VMEM_LIMIT
        ),
        name="experts",
    )(normed, stream, meta, gate_weight[0], up_weight[0], down_weight[0])
    return out.reshape(1, tokens, width)


def solution(mesh):
    tok3 = P("dp", "sp", None)
    tok2 = P("dp", "sp")
    weight = P(("sp", "dp"), None, None)
    placed = (
        tok3, tok3, tok3, tok3, P(), P(), P(), P(), P(), tok3, tok2, tok2, weight, weight, weight,
    )
    return jax.shard_map(
        local, mesh=mesh, in_specs=placed, out_specs=P("dp", "sp", None), check_vma=False
    )
```

profile of v0, /device:TPU:0, one launch (start us, length us, event | category | flops | bytes accessed | tf_op | source)
XLA Modules:
  0.0 105.9 jit_solution(11307440206507037970)
XLA Ops:
  0.0 0.1 pad.3.clone
  0.1 0.7 convert_bitcast_fusion
  0.8 1.3 %maximum_maximum_fusion.meta_ref = f32[8,128]{1,0:T(8,128)} fusion(f32[1,128]{1,0:T(1,128)} %param.28, f32[1,128]{1,0:T(1,128)} %param.27, f32[2,128]{1,0:T(2,128)S(1)} %convert_bitcast_fusion, f32[8]{0:T(128)S(1)} %pad.3.clone), kind=kLoop, calls=%fused_computation | loop fusion | flops 3072 | bytes 6176 | tf_op jit(solution)/shard_map/concatenate | solution.py:491
  2.1 47.1 %attention.1 = (bf16[128,2048]{1,0:T(8,128)(2,1)}, bf16[128,2048]{1,0:T(8,128)(2,1)}) custom-call(bf16[128,2048]{1,0:T(8,128)(2,1)} %bitcast.20, bf16[128,512]{1,0:T(8,128)(2,1)} %bitcast.22, bf16[128,512]{1,0:T(8,128)(2,1)} %bitcast.23, f32[1,128]{1,0:T(1,128)} %bitcast.26, f32[1,128]{1,0:T(1,128)} %bitcast.27, f32[1024,128]{1,0:T(8,128)} %constant.6.clone.cos_ref, ...), custom_call_target="tpu_custom_call" | custom-call | tf_op jit(solution)/shard_map/attention/pallas_call | solution.py:457
  49.2 54.8 %experts.1 = bf16[128,2048]{1,0:T(8,128)(2,1)} custom-call(bf16[128,2048]{1,0:T(8,128)(2,1)} %get-tuple-element.7.normed_ref, bf16[128,2048]{1,0:T(8,128)(2,1)} %get-tuple-element.8.stream_ref, f32[8,128]{1,0:T(8,128)} %maximum_maximum_fusion.meta_ref, bf16[2048,512]{1,0:T(8,128)(2,1)} %bitcast.16, bf16[2048,512]{1,0:T(8,128)(2,1)} %bitcast.17, ...), custom_call_target="tpu_custom_call" | custom-call | tf_op jit(solution)/shard_map/experts/pallas_call | solution.py:496
  104.0 1.9 %copy.19 = bf16[1,128,2048]{2,1,0:T(8,128)(2,1)} copy(bf16[1,128,2048]{2,1,0:T(8,128)(2,1)} %bitcast.19) | data formatting | bytes 1048576
  (1 shorter events, 0.0 us)
where the time goes:
time: 108 us; the launch traced here: 106 us
  Pallas kernels  102 us (94%)
  other arithmetic  2.01 us (2%)
  local copies, waits for them, and re-layouts  1.96 us (2%)
    pallas_call x1, Pallas kernels, local(): pl.pallas_call(functools.partial(expert_kernel, nz, nx, n_dp), out_shape=...  54.8 us
    pallas_call x1, Pallas kernels, local(): pl.pallas_call(functools.partial(attention_kernel, nz, nx), out_shape=(ro...  47.1 us

commit v1 on v0

--- a/solution.py
+++ b/solution.py
@@ -519,6 +519,619 @@
     return out.reshape(1, tokens, width)
 
 
+def layer_kernel(
+    nz, nx, cores,
+    q_ref, k_ref, v_ref, qg_ref, kg_ref, res_ref, post_ref, pre_ref, route_ref, gw_ref, fs_ref,
+    cos_hbm, sin_hbm, ow_hbm, wg_hbm, wu_hbm, wd_hbm,
+    out_ref,
+    kv, q_rot, att, acc, cos, sin, ow, wg, wu, wd, load_sem,
+    rk, sx, su, sd,
+    perm, perm_back, mrow, metas, picks, weights, backs,
+    zs_sem, zr_sem, ms_sem, mr_sem,
+    stream, srt, rows, y, other, part, relay, direct, summed, fin,
+    s1, t1, sxd, tx, syd, ty, sc, tc, so, to, sr, tr, sf, tf, s4, t4,
+):
+    tokens, width = q_ref.shape
+    heads = width // HEAD_DIM
+    kv_heads = k_ref.shape[1] // HEAD_DIM
+    group = heads // kv_heads
+    length = nz * nx * tokens
+    chips = metas.shape[2]
+    count = chips * cores
+    block = tokens // nz
+    cap = y.shape[2] // chips
+    half = block // 2
+    me = lax.axis_index("sp")
+    dp = lax.axis_index("dp")
+    z, x = me // nx, me % nx
+    side, core = dp // cores, dp % cores
+    up, down = (me + nx, dp), (me - nx, dp)
+    beside = (z * nx + 1 - x, dp)
+    across = (me, (1 - side) * cores + core)
+    partner = (me, side * cores + 1 - core)
+    has_up, has_down = z < nz - 1, z > 0
+    mine = side * nx + x
+    chip_x, chip_y = side * nx + 1 - x, (1 - side) * nx + x
+    chip_d = (1 - side) * nx + 1 - x
+
+    def column(plane):
+        return (plane * nx + x, dp)
+
+    flip = z >= nz // 2
+    low = jnp.where(flip, nz - 1 - z, z)
+
+    def source_of(i):
+        if i == 0:
+            return z
+        near = (i - 1) + jnp.where(low <= i - 1, 1, 0)
+        return jnp.where(flip, nz - 1 - near, near)
+
+    sources = [source_of(i) for i in range(nz)]
+
+    own = pl.multiple_of(me * tokens, tokens)
+    loads = [
+        pltpu.make_async_copy(src, dst, load_sem.at[i])
+        for i, (src, dst) in enumerate((
+            (cos_hbm.at[pl.ds(own, tokens)], cos), (sin_hbm.at[pl.ds(own, tokens)], sin),
+            (ow_hbm, ow), (wg_hbm, wg), (wu_hbm, wu), (wd_hbm, wd),
+        ))
+    ]
+    for load in loads:
+        load.start()
+
+    barrier = pltpu.get_barrier_semaphore()
+    greeted = [column(lax.rem(z + dist, nz)) for dist in range(1, nz)] + [beside, across, partner]
+    for device in greeted:
+        pl.semaphore_signal(barrier, inc=1, device_id=device, device_id_type=MESH)
+
+    loads[0].wait()
+    loads[1].wait()
+    for head in range(kv_heads):
+        columns = slice(head * HEAD_DIM, (head + 1) * HEAD_DIM)
+        kv[me, head, 1] = v_ref[:, columns]
+        kv[me, head, 0] = rotate(k_ref[:, columns], kg_ref[...], cos[...], sin[...])
+
+    pl.semaphore_wait(barrier, len(greeted))
+
+    def hop(slot, head, send, device):
+        buf = kv.at[slot, head]
+        return remote(buf, buf, send.at[slot, head], rk.at[slot, head], device)
+
+    def arrived(slot, head):
+        hop(slot, head, sx, up).wait_recv()
+
+    def crossing(head):
+        return lax.rem(head, 2) == 1
+
+    for head in range(kv_heads):
+        hop(me, head, sx, beside).start()
+
+        @pl.when(has_up)
+        def _(head=head):
+            hop(me, head, su, up).start()
+
+        @pl.when(has_down)
+        def _(head=head):
+            hop(me, head, sd, down).start()
+
+    def relay_kv(head):
+        slot_x = z * nx + 1 - x
+        arrived(slot_x, head)
+
+        @pl.when(jnp.logical_and(crossing(head), has_up))
+        def _():
+            hop(slot_x, head, su, up).start()
+
+        @pl.when(jnp.logical_and(crossing(head), has_down))
+        def _():
+            hop(slot_x, head, sd, down).start()
+
+        for dist in range(1, nz):
+            for below in (True, False):
+                source = z - dist if below else z + dist
+                present = source >= 0 if below else source < nz
+                further = has_up if below else has_down
+                onward, send = (up, su) if below else (down, sd)
+
+                @pl.when(present)
+                def _(source=source, further=further, onward=onward, send=send, dist=dist):
+                    slot = source * nx + x
+                    arrived(slot, head)
+
+                    @pl.when(further)
+                    def _():
+                        hop(slot, head, send, onward).start()
+
+                    if dist == 1:
+                        @pl.when(jnp.logical_not(crossing(head)))
+                        def _():
+                            hop(slot, head, sx, beside).start()
+                    else:
+                        hop(slot, head, sx, beside).start()
+
+    for head in range(heads):
+        q_rot[head] = rotate(
+            q_ref[:, head * HEAD_DIM : (head + 1) * HEAD_DIM], qg_ref[...], cos[...], sin[...]
+        )
+    acc[...] = jnp.zeros_like(acc)
+
+    row = lax.broadcasted_iota(jnp.int32, (tokens, tokens), 0)
+    lane = lax.broadcasted_iota(jnp.int32, (tokens, tokens), 1)
+
+    def to_lanes(column_of):
+        return jnp.sum(jnp.where(row == lane, column_of, 0.0), axis=0, keepdims=True)
+
+    def routing():
+        first = route_ref[:, 0:1].astype(F32)
+        second = route_ref[:, 1:2].astype(F32)
+        of = jnp.zeros_like(first)
+        for g in range(1, nz):
+            of = of + jnp.where(first >= float(g * count), 1.0, 0.0)
+        of_lane = to_lanes(of)
+        same = of == of_lane
+        rank = jnp.sum(jnp.where(same & (lane < row), 1.0, 0.0), axis=1, keepdims=True)
+        rank_lane = jnp.sum(jnp.where(same & (row < lane), 1.0, 0.0), axis=0, keepdims=True)
+        place = (of * float(block) + rank).astype(jnp.int32)
+        place_lane = (of_lane * float(block) + rank_lane).astype(jnp.int32)
+        perm[...] = jnp.where(row == place_lane, 1.0, 0.0).astype(BF16)
+        perm_back[...] = jnp.where(place == lane, 1.0, 0.0).astype(BF16)
+        fields = (
+            to_lanes(first), to_lanes(second),
+            gw_ref[...] * fs_ref[...], gw_ref[...] * (1.0 - fs_ref[...]),
+        )
+        chosen = lax.broadcasted_iota(jnp.int32, (8, tokens), 0).astype(F32) == of_lane
+        at = rank.astype(jnp.int32)
+        table = jnp.zeros((8, tokens), F32)
+        for f, field in enumerate(fields):
+            spread = jnp.where(lane == at + f * block, 1.0, 0.0)
+            table += lax.dot_general(
+                jnp.where(chosen, field, 0.0), spread, (((1,), (0,)), ((), ())),
+                precision=lax.Precision.HIGHEST, preferred_element_type=F32,
+            )
+        for g in range(nz):
+            mrow[g] = table[g : g + 1]
+
+    routing()
+    metas[z, core, mine] = mrow[z]
+
+    def meta_column(dist):
+        plane = lax.rem(z + dist, nz)
+        return plane, remote(
+            mrow.at[plane], metas.at[z, core, mine], zs_sem.at[plane], zr_sem.at[z], column(plane)
+        )
+
+    def meta_arrival(dist):
+        plane = lax.rem(z + dist, nz)
+        return remote(
+            mrow.at[plane], metas.at[plane, core, mine], zs_sem.at[plane], zr_sem.at[plane],
+            column(plane),
+        )
+
+    for dist in range(1, nz):
+        meta_column(dist)[1].start()
+
+    def meta_copy(view, step, device):
+        return remote(view, view, ms_sem.at[step], mr_sem.at[step], device)
+
+    pair = pl.ds(side * nx, nx)
+    other_pair = pl.ds((1 - side) * nx, nx)
+    meta_sends = (
+        meta_copy(metas.at[:, core, mine], 0, beside),
+        meta_copy(metas.at[:, core, pair], 1, across),
+        meta_copy(metas.at[:, core], 2, partner),
+    )
+    meta_recvs = (
+        meta_copy(metas.at[:, core, chip_x], 0, beside),
+        meta_copy(metas.at[:, core, other_pair], 1, across),
+        meta_copy(metas.at[:, 1 - core], 2, partner),
+    )
+
+    def choice(plane, of_core, expert):
+        table = metas[plane, of_core].reshape(chips, tokens)
+        first = table[:, 0:block] == expert
+        second = table[:, block : 2 * block] == expert
+        member = jnp.where(first | second, 1.0, 0.0)
+        weight = jnp.where(first, table[:, 2 * block : 3 * block], 0.0)
+        weight = weight + jnp.where(second, table[:, 3 * block : 4 * block], 0.0)
+        r = lax.broadcasted_iota(jnp.int32, (block, block), 0)
+        c = lax.broadcasted_iota(jnp.int32, (block, block), 1)
+        earlier = jnp.where(r < c, 1.0, 0.0).astype(BF16)
+        rank = jnp.dot(
+            jnp.concatenate([member] * (8 // chips), axis=0).astype(BF16), earlier,
+            preferred_element_type=F32,
+        )[:chips]
+        place = lax.broadcasted_iota(jnp.int32, (chips, cap, block), 1).astype(F32)
+        hit = jnp.where(rank[:, None, :] == place, 1.0, 0.0) * member[:, None, :]
+        of_slot = jnp.sum(hit * weight[:, None, :], axis=2, keepdims=True).reshape(chips * cap, 1)
+        flat = hit.reshape(chips * cap, block).astype(BF16)
+        wide_row = lax.broadcasted_iota(jnp.int32, (block, tokens), 0)
+        wide_lane = lax.broadcasted_iota(jnp.int32, (block, tokens), 1)
+        widen = jnp.where(lax.rem(wide_lane, block) == wide_row, 1.0, 0.0).astype(BF16)
+        spread = jnp.dot(flat, widen, preferred_element_type=F32)
+        slot = lax.broadcasted_iota(jnp.int32, (chips * cap, tokens), 0) // cap
+        chip = lax.broadcasted_iota(jnp.int32, (chips * cap, tokens), 1) // block
+        return jnp.where(slot == chip, spread, 0.0), of_slot
+
+    def tables():
+        expert = (z * count + x * (count // nx) + dp).astype(F32)
+        twin = (z * count + x * (count // nx) + side * cores + 1 - core).astype(F32)
+
+        def one_plane(plane, carry):
+            for of_core in range(cores):
+                pick, of_slot = choice(plane, of_core, expert)
+                picks[plane, of_core] = pick.astype(BF16)
+                weights[plane, of_core] = of_slot
+            back, _ = choice(plane, core, expert)
+            theirs, _ = choice(plane, core, twin)
+            backs[plane] = jnp.concatenate([back, theirs], axis=0).T.astype(BF16)
+            return carry
+
+        lax.fori_loop(0, nz, one_plane, 0)
+
+    factor = float(HEAD_DIM**-0.5 * np.log2(np.e))
+    span = group * HEAD_DIM
+
+    def attend(head):
+        keys = kv[:, head, 0].reshape(length, HEAD_DIM)
+        values = kv[:, head, 1].reshape(length, HEAD_DIM)
+        for member in range(group):
+            scores = lax.dot_general(
+                q_rot[head * group + member], keys, (((1,), (1,)), ((), ())),
+                preferred_element_type=F32,
+            )
+            top = jnp.max(scores, axis=-1, keepdims=True)
+            raised = jnp.exp2((scores - top) * factor)
+            total = jnp.sum(raised, axis=-1, keepdims=True)
+            mixed = jnp.dot(raised.astype(BF16), values, preferred_element_type=F32)
+            att[:, member * HEAD_DIM : (member + 1) * HEAD_DIM] = (mixed / total).astype(BF16)
+        above = ow.at[pl.ds(pl.multiple_of(head * span, span), span), :]
+        tile = 1024
+        for start in range(0, width, tile):
+            columns = slice(start, start + tile)
+            acc[:, columns] += jnp.dot(att[...], above[:, columns], preferred_element_type=F32)
+
+    relay_kv(0)
+    loads[2].wait()
+
+    def one_head(head, carry):
+        @pl.when(head + 1 < kv_heads)
+        def _():
+            relay_kv(head + 1)
+
+        @pl.when(head == 0)
+        def _():
+            for dist in range(1, nz):
+                meta_arrival(dist).wait_recv()
+            meta_sends[0].start()
+
+        @pl.when(head == 1)
+        def _():
+            meta_recvs[0].wait_recv()
+            meta_sends[1].start()
+
+        @pl.when(head == 2)
+        def _():
+            meta_recvs[1].wait_recv()
+            meta_sends[2].start()
+
+        @pl.when(head == kv_heads - 1)
+        def _():
+            meta_recvs[2].wait_recv()
+            tables()
+
+        slot_x = 1 - x
+        for dist in range(1, nz):
+            arrived(lax.rem(z + dist, nz) * nx + slot_x, head)
+        attend(head)
+        return carry
+
+    lax.fori_loop(0, kv_heads, one_head, 0)
+
+    blend = acc[...].astype(BF16).astype(F32)
+    blend = blend * lax.rsqrt(jnp.mean(blend * blend, axis=-1, keepdims=True) + EPSILON)
+    flow = (res_ref[...].astype(F32) + blend * post_ref[...]).astype(BF16)
+    stream[...] = flow
+    wide = flow.astype(F32)
+    wide = wide * lax.rsqrt(jnp.mean(wide * wide, axis=-1, keepdims=True) + EPSILON)
+    normed = (wide * pre_ref[...]).astype(BF16)
+    srt[...] = jnp.dot(perm[...], normed, preferred_element_type=F32).astype(BF16).reshape(srt.shape)
+
+    def z_send(plane):
+        return remote(
+            srt.at[plane], rows.at[z, core, mine], s1.at[plane], t1.at[z], column(plane)
+        )
+
+    def z_recv(plane):
+        return remote(
+            srt.at[plane], rows.at[plane, core, mine], s1.at[plane], t1.at[plane], column(plane)
+        )
+
+    for i in range(1, nz):
+        z_send(sources[i]).start()
+    rows[z, core, mine] = srt[z]
+
+    halves = (pl.ds(0, half), pl.ds(half, half))
+
+    def over_x(s, chip, h):
+        view = rows.at[s, core, chip, halves[h]]
+        return remote(view, view, sxd.at[s, chip, h], tx.at[s, chip, h], beside)
+
+    def over_y(s, chip, h):
+        view = rows.at[s, core, chip, halves[h]]
+        return remote(view, view, syd.at[s, chip, h], ty.at[s, chip, h], across)
+
+    def over_core(s, of_core, chip):
+        view = rows.at[s, of_core, chip]
+        return remote(view, view, sc.at[s, chip], tc.at[s, chip], partner)
+
+    def spread_own(i):
+        s = sources[i]
+        if i > 0:
+            z_recv(s).wait_recv()
+        over_x(s, mine, 0).start()
+        over_y(s, mine, 1).start()
+        over_x(s, mine, 1).start()
+        over_y(s, mine, 0).start()
+        over_core(s, core, mine).start()
+
+    def spread_on(i):
+        s = sources[i]
+        over_x(s, chip_x, 0).wait_recv()
+        over_y(s, chip_x, 0).start()
+        over_y(s, chip_y, 1).wait_recv()
+        over_x(s, chip_y, 1).start()
+        over_x(s, chip_x, 1).wait_recv()
+        over_core(s, core, chip_x).start()
+        over_y(s, chip_y, 0).wait_recv()
+        over_core(s, core, chip_y).start()
+
+    def spread_last(i):
+        s = sources[i]
+        over_y(s, chip_d, 0).wait_recv()
+        over_x(s, chip_d, 1).wait_recv()
+        over_core(s, core, chip_d).start()
+
+    def to_partner(s):
+        return remote(y.at[s, 1 - core], other.at[s], so.at[s], to.at[s], partner)
+
+    def transform(i):
+        s = sources[i]
+        for k in range(chips):
+            over_core(s, 1 - core, k).wait_recv()
+        packed = [
+            jnp.dot(
+                picks[s, q], rows[s, q].reshape(tokens, width), preferred_element_type=F32
+            ).astype(BF16)
+            for q in range(cores)
+        ]
+        packed = jnp.concatenate(packed, axis=0)
+        gated = jnp.dot(packed, wg[...], preferred_element_type=F32)
+        lifted = jnp.dot(packed, wu[...], preferred_element_type=F32)
+        hidden = (gated / (1.0 + jnp.exp(-gated)) * lifted).astype(BF16)
+        result = jnp.dot(hidden, wd[...], preferred_element_type=F32)
+        slots = chips * cap
+        for q in range(cores):
+            y[s, q] = (result[q * slots : (q + 1) * slots] * weights[s, q]).astype(BF16)
+        to_partner(s).start()
+
+    def to_relay_y(s):
+        return remote(part.at[s, chip_d, halves[0]], relay.at[s, 0], sr.at[s, 0], tr.at[s, 0], across)
+
+    def to_relay_x(s):
+        return remote(part.at[s, chip_d, halves[1]], relay.at[s, 1], sr.at[s, 1], tr.at[s, 1], beside)
+
+    def direct_x(s):
+        return remote(part.at[s, chip_x, halves[1]], direct.at[s, 1], sr.at[s, 2], tr.at[s, 2], beside)
+
+    def direct_y(s):
+        return remote(part.at[s, chip_y, halves[0]], direct.at[s, 0], sr.at[s, 3], tr.at[s, 3], across)
+
+    def summed_x(s):
+        return remote(part.at[s, chip_x, halves[0]], summed.at[s, 0], sf.at[s, 0], tf.at[s, 0], beside)
+
+    def summed_y(s):
+        return remote(part.at[s, chip_y, halves[1]], summed.at[s, 1], sf.at[s, 1], tf.at[s, 1], across)
+
+    def gather_back(i):
+        s = sources[i]
+        to_partner(s).wait_recv()
+        outs = jnp.concatenate([y[s, core], other[s]], axis=0)
+        part[s] = jnp.dot(backs[s], outs, preferred_element_type=F32).astype(BF16).reshape(
+            chips, block, width
+        )
+        to_relay_y(s).start()
+        to_relay_x(s).start()
+        direct_x(s).start()
+        direct_y(s).start()
+
+    def add(left, right):
+        return (left.astype(F32) + right.astype(F32)).astype(BF16)
+
+    def pass_back(i):
+        s = sources[i]
+        to_relay_y(s).wait_recv()
+        part[s, chip_x, halves[0]] = add(part[s, chip_x, halves[0]], relay[s, 0])
+        summed_x(s).start()
+        to_relay_x(s).wait_recv()
+        part[s, chip_y, halves[1]] = add(part[s, chip_y, halves[1]], relay[s, 1])
+        summed_y(s).start()
+
+    def home(s):
+        return remote(part.at[s, mine], fin.at[z], s4.at[s], t4.at[z], column(s))
+
+    def finish(i):
+        s = sources[i]
+        direct_y(s).wait_recv()
+        summed_x(s).wait_recv()
+        direct_x(s).wait_recv()
+        summed_y(s).wait_recv()
+        for h in range(2):
+            total = part[s, mine, halves[h]].astype(F32) + direct[s, h].astype(F32)
+            total = (total + summed[s, h].astype(F32)).astype(BF16)
+            if i > 0:
+                part[s, mine, halves[h]] = total
+            else:
+                fin[s, halves[h]] = total
+        if i > 0:
+            home(s).start()
+
+    def weights_ready(i):
+        for load in loads[3:]:
+            load.wait()
+
+    for stage, i in plan(
+        spread_own, spread_on, spread_last, weights_ready, transform, gather_back, pass_back, finish
+    ):
+        stage(i)
+
+    for i in range(1, nz):
+        s = sources[i]
+        remote(part.at[s, mine], fin.at[s], s4.at[s], t4.at[s], column(s)).wait_recv()
+    added = jnp.dot(
+        perm_back[...], fin[...].reshape(tokens, width), preferred_element_type=F32
+    )
+    out_ref[...] = (stream[...].astype(F32) + added).astype(BF16)
+
+    def drain_kv(head, carry):
+        for plane in range(nz):
+            slot = plane * nx + x
+
+            @pl.when(jnp.logical_and(has_up, z >= plane))
+            def _(slot=slot):
+                hop(slot, head, su, up).wait_send()
+
+            @pl.when(jnp.logical_and(has_down, z <= plane))
+            def _(slot=slot):
+                hop(slot, head, sd, down).wait_send()
+
+            adjacent = jnp.logical_or(z == plane + 1, z == plane - 1)
+
+            @pl.when(jnp.logical_not(jnp.logical_and(adjacent, crossing(head))))
+            def _(slot=slot):
+                hop(slot, head, sx, beside).wait_send()
+
+        slot_x = z * nx + 1 - x
+
+        @pl.when(jnp.logical_and(crossing(head), has_up))
+        def _():
+            hop(slot_x, head, su, up).wait_send()
+
+        @pl.when(jnp.logical_and(crossing(head), has_down))
+        def _():
+            hop(slot_x, head, sd, down).wait_send()
+
+        return carry
+
+    lax.fori_loop(0, kv_heads, drain_kv, 0)
+    for dist in range(1, nz):
+        meta_column(dist)[1].wait_send()
+    for send in meta_sends:
+        send.wait_send()
+
+    def drain(s, carry):
+        for h in range(2):
+            over_x(s, mine, h).wait_send()
+            over_y(s, mine, h).wait_send()
+        over_y(s, chip_x, 0).wait_send()
+        over_x(s, chip_y, 1).wait_send()
+        for k in range(chips):
+            over_core(s, core, k).wait_send()
+        to_partner(s).wait_send()
+        for copy in (to_relay_y, to_relay_x, direct_x, direct_y, summed_x, summed_y):
+            copy(s).wait_send()
+        return carry
+
+    lax.fori_loop(0, nz, drain, 0)
+    for i in range(1, nz):
+        z_send(sources[i]).wait_send()
+        home(sources[i]).wait_send()
+
+
+def plan(own, on, last, ready, transform, gather_back, pass_back, finish):
+    return (
+        (own, 0), (on, 0), (own, 1), (last, 0), (on, 1), (own, 2), (ready, 0),
+        (transform, 0), (last, 1), (on, 2), (own, 3),
+        (transform, 1), (last, 2), (on, 3), (gather_back, 1),
+        (transform, 2), (last, 3), (gather_back, 2), (pass_back, 1),
+        (transform, 3), (gather_back, 0), (finish, 1), (pass_back, 2), (gather_back, 3),
+        (finish, 2), (pass_back, 3), (pass_back, 0), (finish, 3), (finish, 0),
+    )
+
+
+def fused(
+    residual_in, query_proj, key_proj, value_proj, query_gain, key_gain, out_weight, post_gain,
+    pre_gain, route_ids, group_weight, first_share, gate_weight, up_weight, down_weight,
+):
+    n_sp = lax.axis_size("sp")
+    n_dp = lax.axis_size("dp")
+    tokens, width = query_proj.shape[1:]
+    kv_heads = key_proj.shape[2] // HEAD_DIM
+    heads = width // HEAD_DIM
+    nz = GROUPS
+    nx = n_sp // nz
+    cores = 2
+    chips = nx * (n_dp // cores)
+    experts = gate_weight.shape[0] * n_sp * n_dp
+    cap = max(16, 4 * tokens // experts)
+    block = tokens // nz
+    slots = chips * cap
+    ff = gate_weight.shape[2]
+    length = n_sp * tokens
+    cos, sin = angle_tables(length)
+    vmem = pl.BlockSpec(memory_space=pltpu.VMEM)
+    hbm = pl.BlockSpec(memory_space=pl.ANY)
+    dma = pltpu.SemaphoreType.DMA
+
+    def buf(*shape, kind=BF16):
+        return pltpu.VMEM(shape, kind)
+
+    out = pl.pallas_call(
+        functools.partial(layer_kernel, nz, nx, cores),
+        out_shape=jax.ShapeDtypeStruct((tokens, width), BF16),
+        in_specs=[vmem] * 11 + [hbm] * 6,
+        out_specs=vmem,
+        scratch_shapes=[
+            buf(n_sp, kv_heads, 2, tokens, HEAD_DIM),
+            buf(heads, tokens, HEAD_DIM),
+            buf(tokens, width // kv_heads),
+            buf(tokens, width, kind=F32),
+            buf(tokens, HEAD_DIM, kind=F32), buf(tokens, HEAD_DIM, kind=F32),
+            buf(width, width), buf(width, ff), buf(width, ff), buf(ff, width),
+            dma((6,)),
+            dma((n_sp, kv_heads)), dma((n_sp, kv_heads)), dma((n_sp, kv_heads)),
+            dma((n_sp, kv_heads)),
+            buf(tokens, tokens), buf(tokens, tokens),
+            buf(nz, 1, tokens, kind=F32), buf(nz, cores, chips, 1, tokens, kind=F32),
+            buf(nz, cores, slots, tokens), buf(nz, cores, slots, 1, kind=F32),
+            buf(nz, tokens, cores * slots),
+            dma((nz,)), dma((nz,)), dma((3,)), dma((3,)),
+            buf(tokens, width), buf(nz, block, width), buf(nz, cores, chips, block, width),
+            buf(nz, cores, slots, width), buf(nz, slots, width),
+            buf(nz, chips, block, width),
+            buf(nz, 2, block // 2, width), buf(nz, 2, block // 2, width),
+            buf(nz, 2, block // 2, width), buf(nz, block, width),
+            dma((nz,)), dma((nz,)),
+            dma((nz, chips, 2)), dma((nz, chips, 2)), dma((nz, chips, 2)), dma((nz, chips, 2)),
+            dma((nz, chips)), dma((nz, chips)),
+            dma((nz,)), dma((nz,)),
+            dma((nz, 4)), dma((nz, 4)), dma((nz, 2)), dma((nz, 2)),
+            dma((nz,)), dma((nz,)),
+        ],
+        compiler_params=pltpu.CompilerParams(
+            collective_id=0, has_side_effects=True, vmem_limit_bytes=VMEM_LIMIT
+        ),
+        name="layer",
+    )(
+        query_proj[0], key_proj[0], value_proj[0],
+        query_gain.reshape(1, -1), key_gain.reshape(1, -1),
+        residual_in[0], post_gain.reshape(1, -1), pre_gain.reshape(1, -1),
+        route_ids[0], group_weight, first_share,
+        jnp.asarray(cos), jnp.asarray(sin), out_weight,
+        gate_weight[0], up_weight[0], down_weight[0],
+    )
+    return out.reshape(1, tokens, width)
+
+
 def solution(mesh):
     tok3 = P("dp", "sp", None)
     tok2 = P("dp", "sp")
@@ -526,6 +1139,7 @@
     placed = (
         tok3, tok3, tok3, tok3, P(), P(), P(), P(), P(), tok3, tok2, tok2, weight, weight, weight,
     )
+    small = mesh.shape["sp"] == 2 * GROUPS and mesh.shape["dp"] == 4
     return jax.shard_map(
-        local, mesh=mesh, in_specs=placed, out_specs=P("dp", "sp", None), check_vma=False
+        fused if small else local, mesh=mesh, in_specs=placed, out_specs=P("dp", "sp", None), check_vma=False
     )

time: 108 us -> 94.5 us (0.88); the launches traced: 106 us -> 94.3 us
  Pallas kernels: 102 us -> 91 us
  other arithmetic: 2.01 us -> 0 us
  local copies, waits for them, and re-layouts: 1.96 us -> 3.29 us
    pallas_call x2 -> x1, Pallas kernels: 102 us -> 91 us  [fused(): pl.pallas_call(functools.partial(layer_kernel, nz, nx, cores), out_shape=...]
    unnamed x1 -> x2, local copies, waits for them, and re-layouts: 1.88 us -> 3.29 us
    concatenate x1 -> x0, other arithmetic: 1.33 us -> none  [local(): jnp.concatenate([route_ids[0].T.astype(F32), group_weight, first_share, j...]
where the time goes in v1:
time: 94.5 us; the launch traced here: 94.3 us
  Pallas kernels  91 us (96%)
  local copies, waits for them, and re-layouts  3.29 us (3%)
    pallas_call x1, Pallas kernels, fused(): pl.pallas_call(functools.partial(layer_kernel, nz, nx, cores), out_shape=...  91 us
    unnamed x2, local copies, waits for them, and re-layouts  3.29 us

profile of v1, /device:TPU:0, one launch (start us, length us, event | category | flops | bytes accessed | tf_op | source)
XLA Modules:
  0.0 94.3 jit_solution(9408378567001858683)
XLA Ops:
  0.0 1.4 %copy.18 = s32[1,128,2]{2,1,0:T(8,128)} copy(s32[1,128,2]{1,2,0:T(2,128)} %param.26) | data formatting | bytes 2048 | tf_op args[9]
  1.4 91.0 %layer.1 = bf16[128,2048]{1,0:T(8,128)(2,1)} custom-call(bf16[128,2048]{1,0:T(8,128)(2,1)} %bitcast.17, bf16[128,512]{1,0:T(8,128)(2,1)} %bitcast.20, bf16[128,512]{1,0:T(8,128)(2,1)} %bitcast.21, f32[1,128]{1,0:T(1,128)} %bitcast.24, f32[1,128]{1,0:T(1,128)} %bitcast.25, bf16[128,2048]{1,0:T(8,128)(2,1)} %bitcast.18, f32[1,2048]{1,0:T(1,128)} %bitcast.22, ...), custom_call_target="tpu_custom_call" | custom-call | tf_op jit(solution)/shard_map/layer/pallas_call | solution.py:1088
  92.4 1.9 %copy.20 = bf16[1,128,2048]{2,1,0:T(8,128)(2,1)} copy(bf16[1,128,2048]{2,1,0:T(8,128)(2,1)} %bitcast.13) | data formatting | bytes 1048576

commit v2 on v1

--- a/solution.py
+++ b/solution.py
@@ -521,21 +521,26 @@
 
 def layer_kernel(
     nz, nx, cores,
+    q_hbm, k_hbm, v_hbm, qg_hbm, kg_hbm, res_hbm, post_hbm, pre_hbm, route_hbm, gw_hbm, fs_hbm,
+    cos_hbm, sin_hbm, ow_hbm, wg_hbm, wu_hbm, wd_hbm,
+    out_hbm,
     q_ref, k_ref, v_ref, qg_ref, kg_ref, res_ref, post_ref, pre_ref, route_ref, gw_ref, fs_ref,
-    cos_hbm, sin_hbm, ow_hbm, wg_hbm, wu_hbm, wd_hbm,
-    out_ref,
-    kv, q_rot, att, acc, cos, sin, ow, wg, wu, wd, load_sem,
-    rk, sx, su, sd,
+    cos, sin, ow, wg, wu, wd, load_sem,
+    kv, q_rot, att, acc,
+    rk_own, rk_x, rk_z, kv_x_sent, kv_z_sent,
     perm, perm_back, mrow, metas, picks, weights, backs,
     zs_sem, zr_sem, ms_sem, mr_sem,
-    stream, srt, rows, y, other, part, relay, direct, summed, fin,
-    s1, t1, sxd, tx, syd, ty, sc, tc, so, to, sr, tr, sf, tf, s4, t4,
+    stream, srt, rows, y, other, part, relay, direct, summed, fin, out, out_sem,
+    t_z, t_a, t_b, t_c, t_d, t_core, spread_sent,
+    t_other, t_up, t_side, t_last, t_home, back_sent,
 ):
     tokens, width = q_ref.shape
     heads = width // HEAD_DIM
     kv_heads = k_ref.shape[1] // HEAD_DIM
     group = heads // kv_heads
-    length = nz * nx * tokens
+    slots_kv = nz * nx
+    length = slots_kv * tokens
+    last_head = kv_heads - 1
     chips = metas.shape[2]
     count = chips * cores
     block = tokens // nz
@@ -568,87 +573,124 @@
 
     sources = [source_of(i) for i in range(nz)]
 
+    barrier = pltpu.get_barrier_semaphore()
+    greeted = [column(lax.rem(z + dist, nz)) for dist in range(1, nz)] + [beside, across, partner]
+    for device in greeted:
+        pl.semaphore_signal(barrier, inc=1, device_id=device, device_id_type=MESH)
+
     own = pl.multiple_of(me * tokens, tokens)
     loads = [
         pltpu.make_async_copy(src, dst, load_sem.at[i])
         for i, (src, dst) in enumerate((
+            (k_hbm, k_ref), (v_hbm, v_ref), (kg_hbm, kg_ref),
             (cos_hbm.at[pl.ds(own, tokens)], cos), (sin_hbm.at[pl.ds(own, tokens)], sin),
-            (ow_hbm, ow), (wg_hbm, wg), (wu_hbm, wu), (wd_hbm, wd),
+            (q_hbm, q_ref), (qg_hbm, qg_ref), (route_hbm, route_ref), (gw_hbm, gw_ref),
+            (fs_hbm, fs_ref), (ow_hbm, ow), (res_hbm, res_ref), (post_hbm, post_ref),
+            (pre_hbm, pre_ref), (wg_hbm, wg), (wu_hbm, wu), (wd_hbm, wd),
         ))
     ]
     for load in loads:
         load.start()
 
-    barrier = pltpu.get_barrier_semaphore()
-    greeted = [column(lax.rem(z + dist, nz)) for dist in range(1, nz)] + [beside, across, partner]
-    for device in greeted:
-        pl.semaphore_signal(barrier, inc=1, device_id=device, device_id_type=MESH)
-
-    loads[0].wait()
-    loads[1].wait()
+    for load in loads[:5]:
+        load.wait()
     for head in range(kv_heads):
         columns = slice(head * HEAD_DIM, (head + 1) * HEAD_DIM)
-        kv[me, head, 1] = v_ref[:, columns]
-        kv[me, head, 0] = rotate(k_ref[:, columns], kg_ref[...], cos[...], sin[...])
+        kv[head * slots_kv + me, 1] = v_ref[:, columns]
+        kv[head * slots_kv + me, 0] = rotate(k_ref[:, columns], kg_ref[...], cos[...], sin[...])
 
     pl.semaphore_wait(barrier, len(greeted))
 
-    def hop(slot, head, send, device):
-        buf = kv.at[slot, head]
-        return remote(buf, buf, send.at[slot, head], rk.at[slot, head], device)
-
-    def arrived(slot, head):
-        hop(slot, head, sx, up).wait_recv()
+    def hop(slot, head, device, sent, landed):
+        view = kv.at[head * slots_kv + slot]
+        return remote(view, view, sent.at[0], landed, device)
+
+    def bytes_of(units, sent, landed):
+        view = kv.at[pl.ds(0, units)]
+        return remote(view, view, sent, landed, beside)
+
+    def own_beside(head):
+        return hop(me, head, beside, kv_x_sent, rk_own.at[head])
+
+    def pass_beside(slot, head):
+        return hop(slot, head, beside, kv_x_sent, rk_x.at[head])
+
+    def pass_on(slot, source, head, device):
+        return hop(slot, head, device, kv_z_sent, rk_z.at[source, head])
+
+    def cross_on(head, device):
+        return hop(z * nx + 1 - x, head, device, kv_z_sent, rk_x.at[head])
 
     def crossing(head):
         return lax.rem(head, 2) == 1
 
+    late_up, late_down = z == nz - 2, z == 1
+    at_end = jnp.logical_or(z == 0, z == nz - 1)
+
     for head in range(kv_heads):
-        hop(me, head, sx, beside).start()
-
-        @pl.when(has_up)
+        own_beside(head).start()
+        soon_up = has_up if head < last_head else jnp.logical_and(has_up, ~late_up)
+        soon_down = has_down if head < last_head else jnp.logical_and(has_down, ~late_down)
+
+        @pl.when(soon_up)
         def _(head=head):
-            hop(me, head, su, up).start()
-
-        @pl.when(has_down)
+            pass_on(me, z, head, up).start()
+
+        @pl.when(soon_down)
         def _(head=head):
-            hop(me, head, sd, down).start()
-
-    def relay_kv(head):
-        slot_x = z * nx + 1 - x
-        arrived(slot_x, head)
-
-        @pl.when(jnp.logical_and(crossing(head), has_up))
-        def _():
-            hop(slot_x, head, su, up).start()
-
-        @pl.when(jnp.logical_and(crossing(head), has_down))
-        def _():
-            hop(slot_x, head, sd, down).start()
-
-        for dist in range(1, nz):
+            pass_on(me, z, head, down).start()
+
+    def relay_kv(head, before_last):
+        final = head == last_head
+        bytes_of(1, kv_x_sent.at[0], rk_own.at[head]).wait_recv()
+        crosses = crossing(head)
+        for on, late, device in ((has_up, late_up, up), (has_down, late_down, down)):
+            @pl.when(jnp.logical_and(crosses & on, ~(final & late)))
+            def _(device=device):
+                cross_on(head, device).start()
+
+        def step(dist, given):
             for below in (True, False):
                 source = z - dist if below else z + dist
                 present = source >= 0 if below else source < nz
                 further = has_up if below else has_down
-                onward, send = (up, su) if below else (down, sd)
-
-                @pl.when(present)
-                def _(source=source, further=further, onward=onward, send=send, dist=dist):
+                onward = up if below else down
+
+                @pl.when(jnp.logical_and(present, given))
+                def _(source=source, further=further, onward=onward):
                     slot = source * nx + x
-                    arrived(slot, head)
+                    bytes_of(1, kv_z_sent.at[0], rk_z.at[source, head]).wait_recv()
 
                     @pl.when(further)
                     def _():
-                        hop(slot, head, send, onward).start()
+                        pass_on(slot, source, head, onward).start()
 
                     if dist == 1:
-                        @pl.when(jnp.logical_not(crossing(head)))
+                        @pl.when(~crosses)
                         def _():
-                            hop(slot, head, sx, beside).start()
+                            pass_beside(slot, head).start()
                     else:
-                        hop(slot, head, sx, beside).start()
-
+                        pass_beside(slot, head).start()
+
+        step(1, ~(final & at_end))
+        for dist in range(2, nz):
+            @pl.when(final & (at_end if dist == nz - 1 else (dist == nz - 2) & ~at_end))
+            def _():
+                before_last()
+
+            step(dist, True)
+        step(1, final & at_end)
+        for late, device in ((late_up, up), (late_down, down)):
+            @pl.when(final & late)
+            def _(device=device):
+                pass_on(me, z, head, device).start()
+
+                @pl.when(crosses)
+                def _():
+                    cross_on(head, device).start()
+
+    for load in loads[5:10]:
+        load.wait()
     for head in range(heads):
         q_rot[head] = rotate(
             q_ref[:, head * HEAD_DIM : (head + 1) * HEAD_DIM], qg_ref[...], cos[...], sin[...]
@@ -658,16 +700,13 @@
     row = lax.broadcasted_iota(jnp.int32, (tokens, tokens), 0)
     lane = lax.broadcasted_iota(jnp.int32, (tokens, tokens), 1)
 
-    def to_lanes(column_of):
-        return jnp.sum(jnp.where(row == lane, column_of, 0.0), axis=0, keepdims=True)
-
     def routing():
-        first = route_ref[:, 0:1].astype(F32)
-        second = route_ref[:, 1:2].astype(F32)
-        of = jnp.zeros_like(first)
+        first = route_ref[0:1].astype(F32)
+        second = route_ref[1:2].astype(F32)
+        of_lane = jnp.zeros_like(first)
         for g in range(1, nz):
-            of = of + jnp.where(first >= float(g * count), 1.0, 0.0)
-        of_lane = to_lanes(of)
+            of_lane = of_lane + jnp.where(first >= float(g * count), 1.0, 0.0)
+        of = jnp.sum(jnp.where(row == lane, of_lane, 0.0), axis=1, keepdims=True)
         same = of == of_lane
         rank = jnp.sum(jnp.where(same & (lane < row), 1.0, 0.0), axis=1, keepdims=True)
         rank_lane = jnp.sum(jnp.where(same & (row < lane), 1.0, 0.0), axis=0, keepdims=True)
@@ -676,7 +715,7 @@
         perm[...] = jnp.where(row == place_lane, 1.0, 0.0).astype(BF16)
         perm_back[...] = jnp.where(place == lane, 1.0, 0.0).astype(BF16)
         fields = (
-            to_lanes(first), to_lanes(second),
+            first, second,
             gw_ref[...] * fs_ref[...], gw_ref[...] * (1.0 - fs_ref[...]),
         )
         chosen = lax.broadcasted_iota(jnp.int32, (8, tokens), 0).astype(F32) == of_lane
@@ -696,19 +735,16 @@
 
     def meta_column(dist):
         plane = lax.rem(z + dist, nz)
-        return plane, remote(
-            mrow.at[plane], metas.at[z, core, mine], zs_sem.at[plane], zr_sem.at[z], column(plane)
+        return remote(
+            mrow.at[plane], metas.at[z, core, mine], zs_sem.at[0], zr_sem.at[0], column(plane)
         )
 
-    def meta_arrival(dist):
-        plane = lax.rem(z + dist, nz)
-        return remote(
-            mrow.at[plane], metas.at[plane, core, mine], zs_sem.at[plane], zr_sem.at[plane],
-            column(plane),
-        )
+    def meta_all():
+        view = mrow.at[pl.ds(0, nz - 1)]
+        return remote(view, view, zs_sem.at[0], zr_sem.at[0], beside)
 
     for dist in range(1, nz):
-        meta_column(dist)[1].start()
+        meta_column(dist).start()
 
     def meta_copy(view, step, device):
         return remote(view, view, ms_sem.at[step], mr_sem.at[step], device)
@@ -772,8 +808,9 @@
     span = group * HEAD_DIM
 
     def attend(head):
-        keys = kv[:, head, 0].reshape(length, HEAD_DIM)
-        values = kv[:, head, 1].reshape(length, HEAD_DIM)
+        here = pl.ds(head * slots_kv, slots_kv)
+        keys = kv[here, 0].reshape(length, HEAD_DIM)
+        values = kv[here, 1].reshape(length, HEAD_DIM)
         for member in range(group):
             scores = lax.dot_general(
                 q_rot[head * group + member], keys, (((1,), (1,)), ((), ())),
@@ -790,42 +827,37 @@
             columns = slice(start, start + tile)
             acc[:, columns] += jnp.dot(att[...], above[:, columns], preferred_element_type=F32)
 
-    relay_kv(0)
-    loads[2].wait()
+    def prepare():
+        meta_recvs[2].wait_recv()
+        tables()
+
+    relay_kv(jnp.int32(0), prepare)
+    meta_all().wait_recv()
+    meta_sends[0].start()
+    loads[10].wait()
 
     def one_head(head, carry):
         @pl.when(head + 1 < kv_heads)
         def _():
-            relay_kv(head + 1)
+            relay_kv(head + 1, prepare)
 
         @pl.when(head == 0)
-        def _():
-            for dist in range(1, nz):
-                meta_arrival(dist).wait_recv()
-            meta_sends[0].start()
-
-        @pl.when(head == 1)
         def _():
             meta_recvs[0].wait_recv()
             meta_sends[1].start()
 
-        @pl.when(head == 2)
+        @pl.when(head == 1)
         def _():
             meta_recvs[1].wait_recv()
             meta_sends[2].start()
 
-        @pl.when(head == kv_heads - 1)
-        def _():
-            meta_recvs[2].wait_recv()
-            tables()
-
-        slot_x = 1 - x
-        for dist in range(1, nz):
-            arrived(lax.rem(z + dist, nz) * nx + slot_x, head)
+        bytes_of(nz - 1, kv_x_sent.at[0], rk_x.at[head]).wait_recv()
         attend(head)
         return carry
 
     lax.fori_loop(0, kv_heads, one_head, 0)
+    for load in loads[11:14]:
+        load.wait()
 
     blend = acc[...].astype(BF16).astype(F32)
     blend = blend * lax.rsqrt(jnp.mean(blend * blend, axis=-1, keepdims=True) + EPSILON)
@@ -836,71 +868,70 @@
     normed = (wide * pre_ref[...]).astype(BF16)
     srt[...] = jnp.dot(perm[...], normed, preferred_element_type=F32).astype(BF16).reshape(srt.shape)
 
+    def unit(s, of_core, chip, h=0):
+        return ((s * cores + of_core) * chips + chip) * 2 + h
+
+    def units(first, amount):
+        return rows.at[pl.ds(first, amount)]
+
+    def waiting(amount, landed):
+        return remote(units(0, amount), units(0, amount), spread_sent.at[0], landed, partner)
+
     def z_send(plane):
         return remote(
-            srt.at[plane], rows.at[z, core, mine], s1.at[plane], t1.at[z], column(plane)
-        )
-
-    def z_recv(plane):
-        return remote(
-            srt.at[plane], rows.at[plane, core, mine], s1.at[plane], t1.at[plane], column(plane)
+            srt.at[pl.ds(2 * plane, 2)], units(unit(z, core, mine), 2), spread_sent.at[0], t_z.at[z],
+            column(plane),
         )
 
     for i in range(1, nz):
         z_send(sources[i]).start()
-    rows[z, core, mine] = srt[z]
-
-    halves = (pl.ds(0, half), pl.ds(half, half))
-
-    def over_x(s, chip, h):
-        view = rows.at[s, core, chip, halves[h]]
-        return remote(view, view, sxd.at[s, chip, h], tx.at[s, chip, h], beside)
-
-    def over_y(s, chip, h):
-        view = rows.at[s, core, chip, halves[h]]
-        return remote(view, view, syd.at[s, chip, h], ty.at[s, chip, h], across)
-
-    def over_core(s, of_core, chip):
-        view = rows.at[s, of_core, chip]
-        return remote(view, view, sc.at[s, chip], tc.at[s, chip], partner)
+    rows[pl.ds(unit(z, core, mine), 2)] = srt[pl.ds(2 * z, 2)]
+
+    def over(s, chip, h, landed, device):
+        view = rows.at[unit(s, core, chip, h)]
+        return remote(view, view, spread_sent.at[0], landed.at[s], device)
+
+    def over_core(s, chip):
+        view = units(unit(s, core, chip), 2)
+        return remote(view, view, spread_sent.at[0], t_core.at[s], partner)
 
     def spread_own(i):
         s = sources[i]
         if i > 0:
-            z_recv(s).wait_recv()
-        over_x(s, mine, 0).start()
-        over_y(s, mine, 1).start()
-        over_x(s, mine, 1).start()
-        over_y(s, mine, 0).start()
-        over_core(s, core, mine).start()
+            waiting(2, t_z.at[s]).wait_recv()
+        over(s, mine, 0, t_a, beside).start()
+        over(s, mine, 1, t_b, across).start()
+        over(s, mine, 1, t_c, beside).start()
+        over(s, mine, 0, t_c, across).start()
+        over_core(s, mine).start()
 
     def spread_on(i):
         s = sources[i]
-        over_x(s, chip_x, 0).wait_recv()
-        over_y(s, chip_x, 0).start()
-        over_y(s, chip_y, 1).wait_recv()
-        over_x(s, chip_y, 1).start()
-        over_x(s, chip_x, 1).wait_recv()
-        over_core(s, core, chip_x).start()
-        over_y(s, chip_y, 0).wait_recv()
-        over_core(s, core, chip_y).start()
+        waiting(1, t_a.at[s]).wait_recv()
+        over(s, chip_x, 0, t_d, across).start()
+        waiting(1, t_b.at[s]).wait_recv()
+        over(s, chip_y, 1, t_d, beside).start()
+
+    def spread_core(i):
+        s = sources[i]
+        waiting(2, t_c.at[s]).wait_recv()
+        over_core(s, chip_x).start()
+        over_core(s, chip_y).start()
 
     def spread_last(i):
         s = sources[i]
-        over_y(s, chip_d, 0).wait_recv()
-        over_x(s, chip_d, 1).wait_recv()
-        over_core(s, core, chip_d).start()
+        waiting(2, t_d.at[s]).wait_recv()
+        over_core(s, chip_d).start()
 
     def to_partner(s):
-        return remote(y.at[s, 1 - core], other.at[s], so.at[s], to.at[s], partner)
+        return remote(y.at[s, 1 - core], other.at[s], back_sent.at[0], t_other.at[s], partner)
 
     def transform(i):
         s = sources[i]
-        for k in range(chips):
-            over_core(s, 1 - core, k).wait_recv()
+        waiting(2 * chips, t_core.at[s]).wait_recv()
         packed = [
             jnp.dot(
-                picks[s, q], rows[s, q].reshape(tokens, width), preferred_element_type=F32
+                picks[s, q], rows[pl.ds(unit(s, q, 0), 2 * chips)].reshape(tokens, width), preferred_element_type=F32
             ).astype(BF16)
             for q in range(cores)
         ]
@@ -914,23 +945,12 @@
             y[s, q] = (result[q * slots : (q + 1) * slots] * weights[s, q]).astype(BF16)
         to_partner(s).start()
 
-    def to_relay_y(s):
-        return remote(part.at[s, chip_d, halves[0]], relay.at[s, 0], sr.at[s, 0], tr.at[s, 0], across)
-
-    def to_relay_x(s):
-        return remote(part.at[s, chip_d, halves[1]], relay.at[s, 1], sr.at[s, 1], tr.at[s, 1], beside)
-
-    def direct_x(s):
-        return remote(part.at[s, chip_x, halves[1]], direct.at[s, 1], sr.at[s, 2], tr.at[s, 2], beside)
-
-    def direct_y(s):
-        return remote(part.at[s, chip_y, halves[0]], direct.at[s, 0], sr.at[s, 3], tr.at[s, 3], across)
-
-    def summed_x(s):
-        return remote(part.at[s, chip_x, halves[0]], summed.at[s, 0], sf.at[s, 0], tf.at[s, 0], beside)
-
-    def summed_y(s):
-        return remote(part.at[s, chip_y, halves[1]], summed.at[s, 1], sf.at[s, 1], tf.at[s, 1], across)
+    def back(s, chip, h, into, at, landed, device):
+        return remote(
+            part.at[s, chip, halves[h]], into.at[s, at], back_sent.at[0], landed.at[s], device
+        )
+
+    halves = (pl.ds(0, half), pl.ds(half, half))
 
     def gather_back(i):
         s = sources[i]
@@ -939,32 +959,29 @@
         part[s] = jnp.dot(backs[s], outs, preferred_element_type=F32).astype(BF16).reshape(
             chips, block, width
         )
-        to_relay_y(s).start()
-        to_relay_x(s).start()
-        direct_x(s).start()
-        direct_y(s).start()
+        back(s, chip_d, 0, relay, 0, t_up, across).start()
+        back(s, chip_d, 1, relay, 1, t_side, beside).start()
+        back(s, chip_x, 1, direct, 1, t_last, beside).start()
+        back(s, chip_y, 0, direct, 0, t_last, across).start()
 
     def add(left, right):
         return (left.astype(F32) + right.astype(F32)).astype(BF16)
 
     def pass_back(i):
         s = sources[i]
-        to_relay_y(s).wait_recv()
+        waiting(1, t_up.at[s]).wait_recv()
         part[s, chip_x, halves[0]] = add(part[s, chip_x, halves[0]], relay[s, 0])
-        summed_x(s).start()
-        to_relay_x(s).wait_recv()
+        back(s, chip_x, 0, summed, 0, t_last, beside).start()
+        waiting(1, t_side.at[s]).wait_recv()
         part[s, chip_y, halves[1]] = add(part[s, chip_y, halves[1]], relay[s, 1])
-        summed_y(s).start()
+        back(s, chip_y, 1, summed, 1, t_last, across).start()
 
     def home(s):
-        return remote(part.at[s, mine], fin.at[z], s4.at[s], t4.at[z], column(s))
+        return remote(part.at[s, mine], fin.at[z], back_sent.at[0], t_home.at[0], column(s))
 
     def finish(i):
         s = sources[i]
-        direct_y(s).wait_recv()
-        summed_x(s).wait_recv()
-        direct_x(s).wait_recv()
-        summed_y(s).wait_recv()
+        waiting(4, t_last.at[s]).wait_recv()
         for h in range(2):
             total = part[s, mine, halves[h]].astype(F32) + direct[s, h].astype(F32)
             total = (total + summed[s, h].astype(F32)).astype(BF16)
@@ -976,85 +993,58 @@
             home(s).start()
 
     def weights_ready(i):
-        for load in loads[3:]:
+        for load in loads[14:]:
             load.wait()
 
     for stage, i in plan(
-        spread_own, spread_on, spread_last, weights_ready, transform, gather_back, pass_back, finish
+        spread_own, spread_on, spread_core, spread_last, weights_ready, transform, gather_back, pass_back, finish
     ):
         stage(i)
 
-    for i in range(1, nz):
-        s = sources[i]
-        remote(part.at[s, mine], fin.at[s], s4.at[s], t4.at[s], column(s)).wait_recv()
-    added = jnp.dot(
-        perm_back[...], fin[...].reshape(tokens, width), preferred_element_type=F32
-    )
-    out_ref[...] = (stream[...].astype(F32) + added).astype(BF16)
-
-    def drain_kv(head, carry):
-        for plane in range(nz):
-            slot = plane * nx + x
-
-            @pl.when(jnp.logical_and(has_up, z >= plane))
-            def _(slot=slot):
-                hop(slot, head, su, up).wait_send()
-
-            @pl.when(jnp.logical_and(has_down, z <= plane))
-            def _(slot=slot):
-                hop(slot, head, sd, down).wait_send()
-
-            adjacent = jnp.logical_or(z == plane + 1, z == plane - 1)
-
-            @pl.when(jnp.logical_not(jnp.logical_and(adjacent, crossing(head))))
-            def _(slot=slot):
-                hop(slot, head, sx, beside).wait_send()
-
-        slot_x = z * nx + 1 - x
-
-        @pl.when(jnp.logical_and(crossing(head), has_up))
-        def _():
-            hop(slot_x, head, su, up).wait_send()
-
-        @pl.when(jnp.logical_and(crossing(head), has_down))
-        def _():
-            hop(slot_x, head, sd, down).wait_send()
-
-        return carry
-
-    lax.fori_loop(0, kv_heads, drain_kv, 0)
-    for dist in range(1, nz):
-        meta_column(dist)[1].wait_send()
+    waiting(2 * (nz - 1), t_home.at[0]).wait_recv()
+    tile = width // 4
+    stores = []
+    for n, start in enumerate(range(0, width, tile)):
+        columns = slice(start, start + tile)
+        added = jnp.dot(
+            perm_back[...], fin[:, :, columns].reshape(tokens, tile), preferred_element_type=F32
+        )
+        out[:, columns] = (stream[:, columns].astype(F32) + added).astype(BF16)
+        store = pltpu.make_async_copy(out.at[:, columns], out_hbm.at[:, columns], out_sem.at[n])
+        store.start()
+        stores.append(store)
+
+    for plane in range(nz):
+        lanes = sum(head % 2 for head in range(kv_heads))
+        upward = (plane + 1) * kv_heads + lanes if plane < nz - 1 else 0
+        downward = (nz - plane) * kv_heads + lanes if plane > 0 else 0
+        sideways = nz * kv_heads - lanes * sum(0 <= plane + d < nz for d in (-1, 1))
+
+        @pl.when(z == plane)
+        def _(vertical=upward + downward, sideways=sideways):
+            bytes_of(vertical, kv_z_sent.at[0], rk_own.at[0]).wait_send()
+            bytes_of(sideways, kv_x_sent.at[0], rk_own.at[0]).wait_send()
+
+    meta_all().wait_send()
     for send in meta_sends:
         send.wait_send()
-
-    def drain(s, carry):
-        for h in range(2):
-            over_x(s, mine, h).wait_send()
-            over_y(s, mine, h).wait_send()
-        over_y(s, chip_x, 0).wait_send()
-        over_x(s, chip_y, 1).wait_send()
-        for k in range(chips):
-            over_core(s, core, k).wait_send()
-        to_partner(s).wait_send()
-        for copy in (to_relay_y, to_relay_x, direct_x, direct_y, summed_x, summed_y):
-            copy(s).wait_send()
-        return carry
-
-    lax.fori_loop(0, nz, drain, 0)
-    for i in range(1, nz):
-        z_send(sources[i]).wait_send()
-        home(sources[i]).wait_send()
-
-
-def plan(own, on, last, ready, transform, gather_back, pass_back, finish):
+    spread_units = 2 * (nz - 1) + nz * (6 + 2 * chips)
+    waiting(spread_units, t_core.at[0]).wait_send()
+    back_units = nz * (2 * chips * cap // block + 6) + 2 * (nz - 1)
+    returned = units(0, back_units)
+    remote(returned, returned, back_sent.at[0], t_core.at[0], partner).wait_send()
+    for store in stores:
+        store.wait()
+
+
+def plan(own, on, share, last, ready, transform, gather_back, pass_back, finish):
     return (
-        (own, 0), (on, 0), (own, 1), (last, 0), (on, 1), (own, 2), (ready, 0),
-        (transform, 0), (last, 1), (on, 2), (own, 3),
-        (transform, 1), (last, 2), (on, 3), (gather_back, 1),
-        (transform, 2), (last, 3), (gather_back, 2), (pass_back, 1),
-        (transform, 3), (gather_back, 0), (finish, 1), (pass_back, 2), (gather_back, 3),
-        (finish, 2), (pass_back, 3), (pass_back, 0), (finish, 3), (finish, 0),
+        (own, 0), (on, 0), (own, 1), (share, 0), (on, 1), (own, 2), (last, 0), (share, 1),
+        (ready, 0), (transform, 0), (on, 2), (own, 3), (last, 1), (share, 2), (transform, 1),
+        (on, 3), (last, 2), (share, 3), (gather_back, 1), (transform, 2), (last, 3),
+        (gather_back, 2), (transform, 3), (gather_back, 3), (pass_back, 2), (pass_back, 3),
+        (finish, 2), (gather_back, 0), (pass_back, 1), (finish, 3), (finish, 1),
+        (pass_back, 0), (finish, 0),
     )
 
 
@@ -1088,34 +1078,35 @@
     out = pl.pallas_call(
         functools.partial(layer_kernel, nz, nx, cores),
         out_shape=jax.ShapeDtypeStruct((tokens, width), BF16),
-        in_specs=[vmem] * 11 + [hbm] * 6,
-        out_specs=vmem,
+        in_specs=[hbm] * 17,
+        out_specs=hbm,
         scratch_shapes=[
-            buf(n_sp, kv_heads, 2, tokens, HEAD_DIM),
+            buf(tokens, width), buf(tokens, kv_heads * HEAD_DIM), buf(tokens, kv_heads * HEAD_DIM),
+            buf(1, HEAD_DIM, kind=F32), buf(1, HEAD_DIM, kind=F32), buf(tokens, width),
+            buf(1, width, kind=F32), buf(1, width, kind=F32),
+            buf(2, tokens, kind=jnp.int32), buf(1, tokens, kind=F32), buf(1, tokens, kind=F32),
+            buf(tokens, HEAD_DIM, kind=F32), buf(tokens, HEAD_DIM, kind=F32),
+            buf(width, width), buf(width, ff), buf(width, ff), buf(ff, width),
+            dma((17,)),
+            buf(kv_heads * n_sp, 2, tokens, HEAD_DIM),
             buf(heads, tokens, HEAD_DIM),
             buf(tokens, width // kv_heads),
             buf(tokens, width, kind=F32),
-            buf(tokens, HEAD_DIM, kind=F32), buf(tokens, HEAD_DIM, kind=F32),
-            buf(width, width), buf(width, ff), buf(width, ff), buf(ff, width),
-            dma((6,)),
-            dma((n_sp, kv_heads)), dma((n_sp, kv_heads)), dma((n_sp, kv_heads)),
-            dma((n_sp, kv_heads)),
+            dma((kv_heads,)), dma((kv_heads,)), dma((nz, kv_heads)), dma((1,)), dma((1,)),
             buf(tokens, tokens), buf(tokens, tokens),
             buf(nz, 1, tokens, kind=F32), buf(nz, cores, chips, 1, tokens, kind=F32),
             buf(nz, cores, slots, tokens), buf(nz, cores, slots, 1, kind=F32),
             buf(nz, tokens, cores * slots),
-            dma((nz,)), dma((nz,)), dma((3,)), dma((3,)),
-            buf(tokens, width), buf(nz, block, width), buf(nz, cores, chips, block, width),
+            dma((1,)), dma((1,)), dma((3,)), dma((3,)),
+            buf(tokens, width), buf(2 * nz, block // 2, width),
+            buf(nz * cores * chips * 2, block // 2, width),
             buf(nz, cores, slots, width), buf(nz, slots, width),
             buf(nz, chips, block, width),
             buf(nz, 2, block // 2, width), buf(nz, 2, block // 2, width),
             buf(nz, 2, block // 2, width), buf(nz, block, width),
-            dma((nz,)), dma((nz,)),
-            dma((nz, chips, 2)), dma((nz, chips, 2)), dma((nz, chips, 2)), dma((nz, chips, 2)),
-            dma((nz, chips)), dma((nz, chips)),
-            dma((nz,)), dma((nz,)),
-            dma((nz, 4)), dma((nz, 4)), dma((nz, 2)), dma((nz, 2)),
-            dma((nz,)), dma((nz,)),
+            buf(tokens, width), dma((4,)),
+            dma((nz,)), dma((nz,)), dma((nz,)), dma((nz,)), dma((nz,)), dma((nz,)), dma((1,)),
+            dma((nz,)), dma((nz,)), dma((nz,)), dma((nz,)), dma((1,)), dma((1,)),
         ],
         compiler_params=pltpu.CompilerParams(
             collective_id=0, has_side_effects=True, vmem_limit_bytes=VMEM_LIMIT
@@ -1125,7 +1116,7 @@
         query_proj[0], key_proj[0], value_proj[0],
         query_gain.reshape(1, -1), key_gain.reshape(1, -1),
         residual_in[0], post_gain.reshape(1, -1), pre_gain.reshape(1, -1),
-        route_ids[0], group_weight, first_share,
+        route_ids[0].T, group_weight, first_share,
         jnp.asarray(cos), jnp.asarray(sin), out_weight,
         gate_weight[0], up_weight[0], down_weight[0],
     )

time: 94.5 us -> 84.4 us (0.89)
  Pallas kernels: 91 us -> 82.3 us
  local copies, waits for them, and re-layouts: 3.29 us -> 1.88 us
    pallas_call x1, Pallas kernels: 91 us -> 82.3 us  [fused(): pl.pallas_call(functools.partial(layer_kernel, nz, nx, cores), out_shape=...]
    unnamed x2 -> x1, local copies, waits for them, and re-layouts: 3.29 us -> 1.88 us
where the time goes in v2:
time: 84.4 us; the launch traced here: 84.2 us
  Pallas kernels  82.3 us (98%)
  local copies, waits for them, and re-layouts  1.88 us (2%)
    pallas_call x1, Pallas kernels, fused(): pl.pallas_call(functools.partial(layer_kernel, nz, nx, cores), out_shape=...  82.3 us
    unnamed x1, local copies, waits for them, and re-layouts  1.88 us

profile of v2, /device:TPU:0, one launch (start us, length us, event | category | flops | bytes accessed | tf_op | source)
XLA Modules:
  0.0 84.2 jit_solution(14392324476058042510)
XLA Ops:
  0.0 82.3 %layer.1 = bf16[128,2048]{1,0:T(8,128)(2,1)} custom-call(bf16[128,2048]{1,0:T(8,128)(2,1)} %bitcast.19, bf16[128,512]{1,0:T(8,128)(2,1)} %bitcast.21, bf16[128,512]{1,0:T(8,128)(2,1)} %bitcast.22, f32[1,128]{1,0:T(1,128)} %bitcast.26, f32[1,128]{1,0:T(1,128)} %bitcast.27, bf16[128,2048]{1,0:T(8,128)(2,1)} %bitcast.20, f32[1,2048]{1,0:T(1,128)} %bitcast.23, ...), custom_call_target="tpu_custom_call" | custom-call | tf_op jit(solution)/shard_map/layer/pallas_call | solution.py:1078
  82.3 1.9 %copy.19 = bf16[1,128,2048]{2,1,0:T(8,128)(2,1)} copy(bf16[1,128,2048]{2,1,0:T(8,128)(2,1)} %bitcast.15) | data formatting | bytes 1048576

commit v3 on v2

--- a/solution.py
+++ b/solution.py
@@ -555,20 +555,22 @@
     across = (me, (1 - side) * cores + core)
     partner = (me, side * cores + 1 - core)
     has_up, has_down = z < nz - 1, z > 0
-    mine = side * nx + x
-    chip_x, chip_y = side * nx + 1 - x, (1 - side) * nx + x
-    chip_d = (1 - side) * nx + 1 - x
+    sides = chips // nx
+    mine = x * sides + side
+    chip_x, chip_y = (1 - x) * sides + side, x * sides + 1 - side
+    chip_d = (1 - x) * sides + 1 - side
 
     def column(plane):
         return (plane * nx + x, dp)
 
     flip = z >= nz // 2
     low = jnp.where(flip, nz - 1 - z, z)
+    inner = (2, 0, 3)
 
     def source_of(i):
         if i == 0:
             return z
-        near = (i - 1) + jnp.where(low <= i - 1, 1, 0)
+        near = jnp.where(low == 0, i, inner[i - 1])
         return jnp.where(flip, nz - 1 - near, near)
 
     sources = [source_of(i) for i in range(nz)]
@@ -621,73 +623,72 @@
     def cross_on(head, device):
         return hop(z * nx + 1 - x, head, device, kv_z_sent, rk_x.at[head])
 
-    def crossing(head):
-        return lax.rem(head, 2) == 1
-
     late_up, late_down = z == nz - 2, z == 1
     at_end = jnp.logical_or(z == 0, z == nz - 1)
 
-    for head in range(kv_heads):
+    def send_own(head):
+        final = head == last_head
         own_beside(head).start()
-        soon_up = has_up if head < last_head else jnp.logical_and(has_up, ~late_up)
-        soon_down = has_down if head < last_head else jnp.logical_and(has_down, ~late_down)
-
-        @pl.when(soon_up)
-        def _(head=head):
-            pass_on(me, z, head, up).start()
-
-        @pl.when(soon_down)
-        def _(head=head):
-            pass_on(me, z, head, down).start()
-
-    def relay_kv(head, before_last):
+        for on, late, device in ((has_up, late_up, up), (has_down, late_down, down)):
+            @pl.when(on & ~late if final else on)
+            def _(device=device):
+                pass_on(me, z, head, device).start()
+
+    def take_own(head):
+        bytes_of(1, kv_x_sent.at[0], rk_own.at[head]).wait_recv()
+
+    def crosses(head):
+        return head % 2 == 1
+
+    def cross(head):
         final = head == last_head
-        bytes_of(1, kv_x_sent.at[0], rk_own.at[head]).wait_recv()
-        crosses = crossing(head)
+        take_own(head)
         for on, late, device in ((has_up, late_up, up), (has_down, late_down, down)):
-            @pl.when(jnp.logical_and(crosses & on, ~(final & late)))
+            @pl.when(on & ~late if final else on)
             def _(device=device):
                 cross_on(head, device).start()
 
-        def step(dist, given):
-            for below in (True, False):
-                source = z - dist if below else z + dist
-                present = source >= 0 if below else source < nz
-                further = has_up if below else has_down
-                onward = up if below else down
-
-                @pl.when(jnp.logical_and(present, given))
-                def _(source=source, further=further, onward=onward):
-                    slot = source * nx + x
-                    bytes_of(1, kv_z_sent.at[0], rk_z.at[source, head]).wait_recv()
-
-                    @pl.when(further)
-                    def _():
-                        pass_on(slot, source, head, onward).start()
-
-                    if dist == 1:
-                        @pl.when(~crosses)
-                        def _():
-                            pass_beside(slot, head).start()
-                    else:
-                        pass_beside(slot, head).start()
-
-        step(1, ~(final & at_end))
-        for dist in range(2, nz):
-            @pl.when(final & (at_end if dist == nz - 1 else (dist == nz - 2) & ~at_end))
-            def _():
-                before_last()
-
-            step(dist, True)
-        step(1, final & at_end)
+    def relay_kv(head, dist, given=True):
+        for below in (True, False):
+            source = z - dist if below else z + dist
+            present = source >= 0 if below else source < nz
+            further = has_up if below else has_down
+            onward = up if below else down
+
+            @pl.when(present & given)
+            def _(source=source, further=further, onward=onward):
+                slot = source * nx + x
+                bytes_of(1, kv_z_sent.at[0], rk_z.at[source, head]).wait_recv()
+
+                @pl.when(further)
+                def _():
+                    pass_on(slot, source, head, onward).start()
+
+                if dist > 1 or not crosses(head):
+                    pass_beside(slot, head).start()
+
+    def send_late(head):
         for late, device in ((late_up, up), (late_down, down)):
-            @pl.when(final & late)
+            @pl.when(late)
             def _(device=device):
                 pass_on(me, z, head, device).start()
-
-                @pl.when(crosses)
-                def _():
+                if crosses(head):
                     cross_on(head, device).start()
+
+    def wave(step):
+        for dist in range(1, nz):
+            head = step - (dist - 1)
+            if 0 <= head < kv_heads:
+                relay_kv(head, dist, ~at_end if head == last_head and dist == 1 else True)
+                if dist == 1 and crosses(head):
+                    cross(head)
+        if step == kv_heads + nz - 4:
+            send_late(last_head)
+        if step + 2 < kv_heads:
+            send_own(step + 2)
+
+    for head in range(2):
+        send_own(head)
 
     for load in loads[5:10]:
         load.wait()
@@ -749,17 +750,17 @@
     def meta_copy(view, step, device):
         return remote(view, view, ms_sem.at[step], mr_sem.at[step], device)
 
-    pair = pl.ds(side * nx, nx)
-    other_pair = pl.ds((1 - side) * nx, nx)
+    pair = pl.ds(x * sides, sides)
+    other_pair = pl.ds((1 - x) * sides, sides)
     meta_sends = (
-        meta_copy(metas.at[:, core, mine], 0, beside),
-        meta_copy(metas.at[:, core, pair], 1, across),
-        meta_copy(metas.at[:, core], 2, partner),
+        meta_copy(metas.at[:, core, mine], 0, across),
+        meta_copy(metas.at[:, core, pair], 1, partner),
+        meta_copy(metas.at[:, :, pair], 2, beside),
     )
     meta_recvs = (
-        meta_copy(metas.at[:, core, chip_x], 0, beside),
-        meta_copy(metas.at[:, core, other_pair], 1, across),
-        meta_copy(metas.at[:, 1 - core], 2, partner),
+        meta_copy(metas.at[:, core, chip_y], 0, across),
+        meta_copy(metas.at[:, 1 - core, pair], 1, partner),
+        meta_copy(metas.at[:, :, other_pair], 2, beside),
     )
 
     def choice(plane, of_core, expert):
@@ -827,29 +828,31 @@
             columns = slice(start, start + tile)
             acc[:, columns] += jnp.dot(att[...], above[:, columns], preferred_element_type=F32)
 
-    def prepare():
-        meta_recvs[2].wait_recv()
-        tables()
-
-    relay_kv(jnp.int32(0), prepare)
+    wave(0)
+    wave(1)
     meta_all().wait_recv()
     meta_sends[0].start()
+    wave(2)
+    meta_recvs[0].wait_recv()
+    meta_sends[1].start()
+    meta_recvs[1].wait_recv()
+    meta_sends[2].start()
     loads[10].wait()
+    wave(3)
+    wave(4)
 
     def one_head(head, carry):
-        @pl.when(head + 1 < kv_heads)
-        def _():
-            relay_kv(head + 1, prepare)
-
-        @pl.when(head == 0)
-        def _():
-            meta_recvs[0].wait_recv()
-            meta_sends[1].start()
-
         @pl.when(head == 1)
         def _():
-            meta_recvs[1].wait_recv()
-            meta_sends[2].start()
+            wave(5)
+
+        @pl.when(head == 2)
+        def _():
+            relay_kv(last_head, 1, at_end)
+
+        @pl.when(lax.rem(head, 2) == 0)
+        def _():
+            take_own(head)
 
         bytes_of(nz - 1, kv_x_sent.at[0], rk_x.at[head]).wait_recv()
         attend(head)
@@ -883,8 +886,12 @@
             column(plane),
         )
 
-    for i in range(1, nz):
-        z_send(sources[i]).start()
+    z_send(sources[1]).start()
+
+    @pl.when(~at_end)
+    def _():
+        z_send(sources[2]).start()
+
     rows[pl.ds(unit(z, core, mine), 2)] = srt[pl.ds(2 * z, 2)]
 
     def over(s, chip, h, landed, device):
@@ -894,6 +901,16 @@
     def over_core(s, chip):
         view = units(unit(s, core, chip), 2)
         return remote(view, view, spread_sent.at[0], t_core.at[s], partner)
+
+    def route_tables(i):
+        z_send(jnp.where(at_end, sources[2], sources[3])).start()
+        meta_recvs[2].wait_recv()
+        tables()
+
+    def send_far(i):
+        @pl.when(at_end)
+        def _():
+            z_send(sources[i]).start()
 
     def spread_own(i):
         s = sources[i]
@@ -997,7 +1014,7 @@
             load.wait()
 
     for stage, i in plan(
-        spread_own, spread_on, spread_core, spread_last, weights_ready, transform, gather_back, pass_back, finish
+        route_tables, send_far, spread_own, spread_on, spread_core, spread_last, weights_ready, transform, gather_back, pass_back, finish
     ):
         stage(i)
 
@@ -1037,14 +1054,14 @@
         store.wait()
 
 
-def plan(own, on, share, last, ready, transform, gather_back, pass_back, finish):
+def plan(route, far, own, on, share, last, ready, transform, gather_back, pass_back, finish):
     return (
-        (own, 0), (on, 0), (own, 1), (share, 0), (on, 1), (own, 2), (last, 0), (share, 1),
-        (ready, 0), (transform, 0), (on, 2), (own, 3), (last, 1), (share, 2), (transform, 1),
-        (on, 3), (last, 2), (share, 3), (gather_back, 1), (transform, 2), (last, 3),
-        (gather_back, 2), (transform, 3), (gather_back, 3), (pass_back, 2), (pass_back, 3),
-        (finish, 2), (gather_back, 0), (pass_back, 1), (finish, 3), (finish, 1),
-        (pass_back, 0), (finish, 0),
+        (own, 0), (route, 0), (far, 3), (on, 0), (own, 1), (share, 0), (on, 1), (own, 2),
+        (last, 0), (share, 1), (ready, 0), (transform, 0), (on, 2), (own, 3), (last, 1),
+        (share, 2), (transform, 1), (on, 3), (gather_back, 1), (last, 2), (transform, 2),
+        (share, 3), (gather_back, 2), (last, 3), (pass_back, 1), (transform, 3), (pass_back, 2),
+        (finish, 1), (gather_back, 3), (finish, 2), (pass_back, 3), (gather_back, 0),
+        (finish, 3), (pass_back, 0), (finish, 0),
     )
 
 

time: 84.4 us -> 77.1 us (0.914)
  Pallas kernels: 82.3 us -> 75 us
    pallas_call x1, Pallas kernels: 82.3 us -> 75 us  [fused(): pl.pallas_call(functools.partial(layer_kernel, nz, nx, cores), out_shape=...]
where the time goes in v3:
time: 77.1 us; the launch traced here: 76.9 us
  Pallas kernels  75 us (97%)
  local copies, waits for them, and re-layouts  1.88 us (2%)
    pallas_call x1, Pallas kernels, fused(): pl.pallas_call(functools.partial(layer_kernel, nz, nx, cores), out_shape=...  75 us
    unnamed x1, local copies, waits for them, and re-layouts  1.88 us

profile of v3, /device:TPU:0, one launch (start us, length us, event | category | flops | bytes accessed | tf_op | source)
XLA Modules:
  0.0 76.9 jit_solution(7172189350007012671)
XLA Ops:
  0.0 75.0 %layer.1 = bf16[128,2048]{1,0:T(8,128)(2,1)} custom-call(bf16[128,2048]{1,0:T(8,128)(2,1)} %bitcast.19, bf16[128,512]{1,0:T(8,128)(2,1)} %bitcast.21, bf16[128,512]{1,0:T(8,128)(2,1)} %bitcast.22, f32[1,128]{1,0:T(1,128)} %bitcast.26, f32[1,128]{1,0:T(1,128)} %bitcast.27, bf16[128,2048]{1,0:T(8,128)(2,1)} %bitcast.20, f32[1,2048]{1,0:T(1,128)} %bitcast.23, ...), custom_call_target="tpu_custom_call" | custom-call | tf_op jit(solution)/shard_map/layer/pallas_call | solution.py:1095
  75.0 1.9 %copy.19 = bf16[1,128,2048]{2,1,0:T(8,128)(2,1)} copy(bf16[1,128,2048]{2,1,0:T(8,128)(2,1)} %bitcast.15) | data formatting | bytes 1048576

commit v4 on v3

--- a/solution.py
+++ b/solution.py
@@ -519,18 +519,21 @@
     return out.reshape(1, tokens, width)
 
 
+LAYER_VMEM_LIMIT = 50 * 1024 * 1024
+
+
 def layer_kernel(
     nz, nx, cores,
     q_hbm, k_hbm, v_hbm, qg_hbm, kg_hbm, res_hbm, post_hbm, pre_hbm, route_hbm, gw_hbm, fs_hbm,
     cos_hbm, sin_hbm, ow_hbm, wg_hbm, wu_hbm, wd_hbm,
-    out_hbm,
+    out,
     q_ref, k_ref, v_ref, qg_ref, kg_ref, res_ref, post_ref, pre_ref, route_ref, gw_ref, fs_ref,
     cos, sin, ow, wg, wu, wd, load_sem,
-    kv, q_rot, att, acc,
+    kv, q_rot, att, acc, summing,
     rk_own, rk_x, rk_z, kv_x_sent, kv_z_sent,
     perm, perm_back, mrow, metas, picks, weights, backs,
     zs_sem, zr_sem, ms_sem, mr_sem,
-    stream, srt, rows, y, other, part, relay, direct, summed, fin, out, out_sem,
+    stream, srt, rows, y, other, part, relay, direct, summed, fin,
     t_z, t_a, t_b, t_c, t_d, t_core, spread_sent,
     t_other, t_up, t_side, t_last, t_home, back_sent,
 ):
@@ -697,6 +700,7 @@
             q_ref[:, head * HEAD_DIM : (head + 1) * HEAD_DIM], qg_ref[...], cos[...], sin[...]
         )
     acc[...] = jnp.zeros_like(acc)
+    summing[:, HEAD_DIM:] = jnp.ones((length, HEAD_DIM), BF16)
 
     row = lax.broadcasted_iota(jnp.int32, (tokens, tokens), 0)
     lane = lax.broadcasted_iota(jnp.int32, (tokens, tokens), 1)
@@ -811,17 +815,24 @@
     def attend(head):
         here = pl.ds(head * slots_kv, slots_kv)
         keys = kv[here, 0].reshape(length, HEAD_DIM)
-        values = kv[here, 1].reshape(length, HEAD_DIM)
-        for member in range(group):
-            scores = lax.dot_general(
+        summing[:, :HEAD_DIM] = kv[here, 1].reshape(length, HEAD_DIM)
+
+        def scores_of(member):
+            return lax.dot_general(
                 q_rot[head * group + member], keys, (((1,), (1,)), ((), ())),
                 preferred_element_type=F32,
             )
+
+        scores = scores_of(0)
+        for member in range(group):
+            later = scores_of(member + 1) if member + 1 < group else None
             top = jnp.max(scores, axis=-1, keepdims=True)
-            raised = jnp.exp2((scores - top) * factor)
-            total = jnp.sum(raised, axis=-1, keepdims=True)
-            mixed = jnp.dot(raised.astype(BF16), values, preferred_element_type=F32)
-            att[:, member * HEAD_DIM : (member + 1) * HEAD_DIM] = (mixed / total).astype(BF16)
+            raised = jnp.exp2((scores - top) * factor).astype(BF16)
+            mixed = jnp.dot(raised, summing[...], preferred_element_type=F32)
+            att[:, member * HEAD_DIM : (member + 1) * HEAD_DIM] = (
+                mixed[:, :HEAD_DIM] / mixed[:, HEAD_DIM:]
+            ).astype(BF16)
+            scores = later
         above = ow.at[pl.ds(pl.multiple_of(head * span, span), span), :]
         tile = 1024
         for start in range(0, width, tile):
@@ -1020,16 +1031,12 @@
 
     waiting(2 * (nz - 1), t_home.at[0]).wait_recv()
     tile = width // 4
-    stores = []
-    for n, start in enumerate(range(0, width, tile)):
+    for start in range(0, width, tile):
         columns = slice(start, start + tile)
         added = jnp.dot(
             perm_back[...], fin[:, :, columns].reshape(tokens, tile), preferred_element_type=F32
         )
         out[:, columns] = (stream[:, columns].astype(F32) + added).astype(BF16)
-        store = pltpu.make_async_copy(out.at[:, columns], out_hbm.at[:, columns], out_sem.at[n])
-        store.start()
-        stores.append(store)
 
     for plane in range(nz):
         lanes = sum(head % 2 for head in range(kv_heads))
@@ -1050,17 +1057,15 @@
     back_units = nz * (2 * chips * cap // block + 6) + 2 * (nz - 1)
     returned = units(0, back_units)
     remote(returned, returned, back_sent.at[0], t_core.at[0], partner).wait_send()
-    for store in stores:
-        store.wait()
 
 
 def plan(route, far, own, on, share, last, ready, transform, gather_back, pass_back, finish):
     return (
-        (own, 0), (route, 0), (far, 3), (on, 0), (own, 1), (share, 0), (on, 1), (own, 2),
-        (last, 0), (share, 1), (ready, 0), (transform, 0), (on, 2), (own, 3), (last, 1),
+        (own, 0), (route, 0), (far, 3), (on, 0), (own, 1), (share, 0), (on, 1), (last, 0),
+        (own, 2), (share, 1), (ready, 0), (transform, 0), (on, 2), (last, 1), (own, 3),
         (share, 2), (transform, 1), (on, 3), (gather_back, 1), (last, 2), (transform, 2),
-        (share, 3), (gather_back, 2), (last, 3), (pass_back, 1), (transform, 3), (pass_back, 2),
-        (finish, 1), (gather_back, 3), (finish, 2), (pass_back, 3), (gather_back, 0),
+        (share, 3), (pass_back, 1), (gather_back, 2), (last, 3), (transform, 3), (finish, 1),
+        (pass_back, 2), (gather_back, 3), (finish, 2), (pass_back, 3), (gather_back, 0),
         (finish, 3), (pass_back, 0), (finish, 0),
     )
 
@@ -1096,7 +1101,7 @@
         functools.partial(layer_kernel, nz, nx, cores),
         out_shape=jax.ShapeDtypeStruct((tokens, width), BF16),
         in_specs=[hbm] * 17,
-        out_specs=hbm,
+        out_specs=vmem,
         scratch_shapes=[
             buf(tokens, width), buf(tokens, kv_heads * HEAD_DIM), buf(tokens, kv_heads * HEAD_DIM),
             buf(1, HEAD_DIM, kind=F32), buf(1, HEAD_DIM, kind=F32), buf(tokens, width),
@@ -1109,6 +1114,7 @@
             buf(heads, tokens, HEAD_DIM),
             buf(tokens, width // kv_heads),
             buf(tokens, width, kind=F32),
+            buf(length, 2 * HEAD_DIM),
             dma((kv_heads,)), dma((kv_heads,)), dma((nz, kv_heads)), dma((1,)), dma((1,)),
             buf(tokens, tokens), buf(tokens, tokens),
             buf(nz, 1, tokens, kind=F32), buf(nz, cores, chips, 1, tokens, kind=F32),
@@ -1121,22 +1127,21 @@
             buf(nz, chips, block, width),
             buf(nz, 2, block // 2, width), buf(nz, 2, block // 2, width),
             buf(nz, 2, block // 2, width), buf(nz, block, width),
-            buf(tokens, width), dma((4,)),
             dma((nz,)), dma((nz,)), dma((nz,)), dma((nz,)), dma((nz,)), dma((nz,)), dma((1,)),
             dma((nz,)), dma((nz,)), dma((nz,)), dma((nz,)), dma((1,)), dma((1,)),
         ],
         compiler_params=pltpu.CompilerParams(
-            collective_id=0, has_side_effects=True, vmem_limit_bytes=VMEM_LIMIT
+            collective_id=0, has_side_effects=True, vmem_limit_bytes=LAYER_VMEM_LIMIT
         ),
         name="layer",
-    )(
+    )(*(pltpu.with_memory_space_constraint(array, pltpu.HBM) for array in (
         query_proj[0], key_proj[0], value_proj[0],
         query_gain.reshape(1, -1), key_gain.reshape(1, -1),
         residual_in[0], post_gain.reshape(1, -1), pre_gain.reshape(1, -1),
         route_ids[0].T, group_weight, first_share,
         jnp.asarray(cos), jnp.asarray(sin), out_weight,
         gate_weight[0], up_weight[0], down_weight[0],
-    )
+    )))
     return out.reshape(1, tokens, width)
 
 

time: 77.1 us -> 71.4 us (0.926)
  Pallas kernels: 75 us -> 70.4 us
  local copies, waits for them, and re-layouts: 1.88 us -> 0.8 us
    pallas_call x1, Pallas kernels: 75 us -> 70.4 us  [fused(): pl.pallas_call(functools.partial(layer_kernel, nz, nx, cores), out_shape=...]
    unnamed x1, local copies, waits for them, and re-layouts: 1.88 us -> 0.8 us
where the time goes in v4:
time: 71.4 us; the launch traced here: 71.2 us
  Pallas kernels  70.4 us (99%)
  local copies, waits for them, and re-layouts  0.8 us (1%)
    pallas_call x1, Pallas kernels, fused(): pl.pallas_call(functools.partial(layer_kernel, nz, nx, cores), out_shape=...  70.4 us

profile of v4, /device:TPU:0, one launch (start us, length us, event | category | flops | bytes accessed | tf_op | source)
XLA Modules:
  0.0 71.2 jit_solution(8256701048118855798)
XLA Ops:
  0.0 70.4 %layer.1 = bf16[128,2048]{1,0:T(8,128)(2,1)S(1)} custom-call(bf16[128,2048]{1,0:T(8,128)(2,1)} %bitcast.19, bf16[128,512]{1,0:T(8,128)(2,1)} %bitcast.21, bf16[128,512]{1,0:T(8,128)(2,1)} %bitcast.22, f32[1,128]{1,0:T(1,128)} %bitcast.26, f32[1,128]{1,0:T(1,128)} %bitcast.27, bf16[128,2048]{1,0:T(8,128)(2,1)} %bitcast.20, f32[1,2048]{1,0:T(1,128)} %bitcast.23, ...), custom_call_target="tpu_custom_call" | custom-call | tf_op jit(solution)/shard_map/layer/pallas_call | solution.py:1100
  70.4 0.8 %copy.19 = bf16[1,128,2048]{2,1,0:T(8,128)(2,1)} copy(bf16[1,128,2048]{2,1,0:T(8,128)(2,1)S(1)} %bitcast.15) | data formatting | bytes 1048576

commit v5 on v4

--- a/solution.py
+++ b/solution.py
@@ -578,11 +578,6 @@
 
     sources = [source_of(i) for i in range(nz)]
 
-    barrier = pltpu.get_barrier_semaphore()
-    greeted = [column(lax.rem(z + dist, nz)) for dist in range(1, nz)] + [beside, across, partner]
-    for device in greeted:
-        pl.semaphore_signal(barrier, inc=1, device_id=device, device_id_type=MESH)
-
     own = pl.multiple_of(me * tokens, tokens)
     loads = [
         pltpu.make_async_copy(src, dst, load_sem.at[i])
@@ -594,16 +589,23 @@
             (pre_hbm, pre_ref), (wg_hbm, wg), (wu_hbm, wu), (wd_hbm, wd),
         ))
     ]
-    for load in loads:
+    for load in loads[:10]:
         load.start()
+
+    barrier = pltpu.get_barrier_semaphore()
+    greeted = [column(lax.rem(z + dist, nz)) for dist in range(1, nz)] + [beside, across, partner]
+    for device in greeted:
+        pl.semaphore_signal(barrier, inc=1, device_id=device, device_id_type=MESH)
+
 
     for load in loads[:5]:
         load.wait()
-    for head in range(kv_heads):
+    def turn(head):
         columns = slice(head * HEAD_DIM, (head + 1) * HEAD_DIM)
         kv[head * slots_kv + me, 1] = v_ref[:, columns]
         kv[head * slots_kv + me, 0] = rotate(k_ref[:, columns], kg_ref[...], cos[...], sin[...])
 
+    turn(0)
     pl.semaphore_wait(barrier, len(greeted))
 
     def hop(slot, head, device, sent, landed):
@@ -629,13 +631,15 @@
     late_up, late_down = z == nz - 2, z == 1
     at_end = jnp.logical_or(z == 0, z == nz - 1)
 
-    def send_own(head):
-        final = head == last_head
-        own_beside(head).start()
+    def send_along(head, given):
         for on, late, device in ((has_up, late_up, up), (has_down, late_down, down)):
-            @pl.when(on & ~late if final else on)
+            @pl.when((on & ~late if head == last_head else on) & given)
             def _(device=device):
                 pass_on(me, z, head, device).start()
+
+    def send_own(head):
+        own_beside(head).start()
+        send_along(head, True)
 
     def take_own(head):
         bytes_of(1, kv_x_sent.at[0], rk_own.at[head]).wait_recv()
@@ -678,20 +682,30 @@
                 if crosses(head):
                     cross_on(head, device).start()
 
+    def near_wave(head):
+        relay_kv(head, 1, ~at_end if head == last_head else True)
+        if head == 0:
+            send_own(last_head)
+        if crosses(head) and head < last_head:
+            cross(head)
+
     def wave(step):
-        for dist in range(1, nz):
-            head = step - (dist - 1)
+        for dist in range(2, nz):
+            head = step - (dist - 2)
             if 0 <= head < kv_heads:
-                relay_kv(head, dist, ~at_end if head == last_head and dist == 1 else True)
-                if dist == 1 and crosses(head):
-                    cross(head)
-        if step == kv_heads + nz - 4:
-            send_late(last_head)
-        if step + 2 < kv_heads:
-            send_own(step + 2)
-
-    for head in range(2):
-        send_own(head)
+                relay_kv(head, dist)
+            if dist == 2 and head == last_head:
+                send_late(last_head)
+        if step == 1 and crosses(last_head):
+            cross(last_head)
+
+    for head in range(kv_heads):
+        if head > 0:
+            turn(head)
+        if head < last_head:
+            send_own(head)
+    for load in loads[10:]:
+        load.start()
 
     for load in loads[5:10]:
         load.wait()
@@ -839,23 +853,26 @@
             columns = slice(start, start + tile)
             acc[:, columns] += jnp.dot(att[...], above[:, columns], preferred_element_type=F32)
 
+    near_wave(0)
+    near_wave(1)
     wave(0)
+    for head in range(2, kv_heads):
+        near_wave(head)
     wave(1)
     meta_all().wait_recv()
     meta_sends[0].start()
+    loads[10].wait()
     wave(2)
+    wave(3)
     meta_recvs[0].wait_recv()
     meta_sends[1].start()
-    meta_recvs[1].wait_recv()
-    meta_sends[2].start()
-    loads[10].wait()
-    wave(3)
-    wave(4)
 
     def one_head(head, carry):
         @pl.when(head == 1)
         def _():
-            wave(5)
+            wave(4)
+            meta_recvs[1].wait_recv()
+            meta_sends[2].start()
 
         @pl.when(head == 2)
         def _():
@@ -873,13 +890,16 @@
     for load in loads[11:14]:
         load.wait()
 
-    blend = acc[...].astype(BF16).astype(F32)
-    blend = blend * lax.rsqrt(jnp.mean(blend * blend, axis=-1, keepdims=True) + EPSILON)
-    flow = (res_ref[...].astype(F32) + blend * post_ref[...]).astype(BF16)
-    stream[...] = flow
-    wide = flow.astype(F32)
-    wide = wide * lax.rsqrt(jnp.mean(wide * wide, axis=-1, keepdims=True) + EPSILON)
-    normed = (wide * pre_ref[...]).astype(BF16)
+    for start in range(0, tokens, 16):
+        lines = slice(start, start + 16)
+        blend = acc[lines, :].astype(BF16).astype(F32)
+        blend = blend * lax.rsqrt(jnp.mean(blend * blend, axis=-1, keepdims=True) + EPSILON)
+        flow = (res_ref[lines, :].astype(F32) + blend * post_ref[...]).astype(BF16)
+        stream[lines, :] = flow
+        wide = flow.astype(F32)
+        wide = wide * lax.rsqrt(jnp.mean(wide * wide, axis=-1, keepdims=True) + EPSILON)
+        out[lines, :] = (wide * pre_ref[...]).astype(BF16)
+    normed = out[...]
     srt[...] = jnp.dot(perm[...], normed, preferred_element_type=F32).astype(BF16).reshape(srt.shape)
 
     def unit(s, of_core, chip, h=0):

time: 71.4 us -> 70.7 us (level)
    pallas_call x1, Pallas kernels: 70.4 us -> 69.7 us  [fused(): pl.pallas_call(functools.partial(layer_kernel, nz, nx, cores), out_shape=...]
where the time goes in v5:
time: 70.7 us; the launch traced here: 70.5 us
  Pallas kernels  69.7 us (99%)
  local copies, waits for them, and re-layouts  0.8 us (1%)
    pallas_call x1, Pallas kernels, fused(): pl.pallas_call(functools.partial(layer_kernel, nz, nx, cores), out_shape=...  69.7 us

profile of v5, /device:TPU:0, one launch (start us, length us, event | category | flops | bytes accessed | tf_op | source)
XLA Modules:
  0.0 70.5 jit_solution(2342825082935690180)
XLA Ops:
  0.0 69.7 %layer.1 = bf16[128,2048]{1,0:T(8,128)(2,1)S(1)} custom-call(bf16[128,2048]{1,0:T(8,128)(2,1)} %bitcast.19, bf16[128,512]{1,0:T(8,128)(2,1)} %bitcast.21, bf16[128,512]{1,0:T(8,128)(2,1)} %bitcast.22, f32[1,128]{1,0:T(1,128)} %bitcast.26, f32[1,128]{1,0:T(1,128)} %bitcast.27, bf16[128,2048]{1,0:T(8,128)(2,1)} %bitcast.20, f32[1,2048]{1,0:T(1,128)} %bitcast.23, ...), custom_call_target="tpu_custom_call" | custom-call | tf_op jit(solution)/shard_map/layer/pallas_call | solution.py:1120
  69.7 0.8 %copy.19 = bf16[1,128,2048]{2,1,0:T(8,128)(2,1)} copy(bf16[1,128,2048]{2,1,0:T(8,128)(2,1)S(1)} %bitcast.15) | data formatting | bytes 1048576
